TPU v7x, 32 devices: a whole 2x2x4 slice. The times are simulated.
32 devices in a mesh: sp: 16 (over z, y, core), tp: 2 (over x).
Axes of the slice: x: 2, y: 2, z: 4, core: 2. Of those that a mesh axis runs over, the one named last changes fastest.
Arguments:
- layer_source_rows: bfloat16 [6144, 2048], P(('sp', 'tp')), may hold values from -6 to 6
- entry_rescale_factor: bfloat16 [2048], replicated, may hold values from 0.099609375 to 1.8984375
- sliding_mixer_entry_matrix: bfloat16 [3, 2048, 1024], P(None, 'sp', 'tp'), may hold values from -0.125 to 0.125
- recurrent_mixer_entry_matrix: bfloat16 [2, 2048, 1024], P(None, 'sp', 'tp'), may hold values from -0.125 to 0.125
- latent_write_read_matrix: bfloat16 [2, 2048, 2048], P(None, 'sp', 'tp'), may hold values from -0.125 to 0.125
- timestep_matrix: bfloat16 [2048, 2, 16], P(None, None, 'tp'), may hold values from -0.125 to 0.125
- sliding_kernel_coefficients: bfloat16 [3, 1024], P(None, 'tp'), may hold values from -3.5 to 3.5
- recurrent_kernel_coefficients: bfloat16 [5, 1024], P(None, 'tp'), may hold values from -0.5 to 0.5
- latent_kernel_coefficients: bfloat16 [5, 2, 2048], P(None, None, 'tp'), may hold values from -0.5 to 0.5
- lane_forgetting_rate: float32 [2, 16], P(None, 'tp'), may hold values from 0 to 1
- spike_forgetting_rate: float32 [6144, 16], P('sp', 'tp'), may hold values from -2 to 0
- lane_rescale_factor: bfloat16 [1024], P('tp'), may hold values from 0.099609375 to 1.8984375
- sliding_mixer_exit_matrix: bfloat16 [1024, 2048], P('tp', 'sp'), may hold values from -0.125 to 0.125
- recurrent_mixer_exit_matrix: bfloat16 [1024, 2048], P('tp', 'sp'), may hold values from -0.125 to 0.125
Outputs:
- mixed_out: bfloat16 [6144, 2048], P(('sp', 'tp'))
All inputs are finite; a program needn't handle non-finite values.
Results may differ from a plain program's by a relative error of at most 0.017.
Values may be sent and summed in bfloat16 or wider, within the bound.
A program may use at most 64 MiB of HBM per device.

v0:
```python
import functools

import jax
import jax.numpy as jnp
from jax import lax
from jax.experimental import pallas as pl
from jax.experimental.pallas import tpu as pltpu
from jax.sharding import PartitionSpec as P

HEAD_DIM = 64
STATE = 128
HALO = 8
CHUNKS = 2
epsilon = 1e-05
F32 = jnp.float32
BF16 = jnp.bfloat16
HIGHEST = lax.Precision.HIGHEST


def ring_kernel(n, w_ref, out_ref, own_sem, ring_send, ring_recv, mate_send, mate_recv):
    chips = n // 2
    me = lax.axis_index("sp")
    core, chip = me % 2, me // 2
    odd = chip % 2
    spot = (1 - odd) * (chip // 2) + odd * (chips - 1 - chip // 2)

    def device(position):
        position = (position + 2 * chips) % chips
        half = (chips + 1) // 2
        late = position // half
        late_chip = 2 * (chips - 1 - position) + 1
        return 2 * ((1 - late) * 2 * position + late * late_chip) + core

    mate = me + 1 - 2 * core
    ways = (device(spot + 1), device(spot - 1))
    rows = w_ref.shape[0] // (2 * CHUNKS)

    barrier = pltpu.get_barrier_semaphore()
    for other in (mate,) + ways:
        pl.semaphore_signal(
            barrier, inc=1, device_id={"sp": other}, device_id_type=pl.DeviceIdType.MESH
        )
    pl.semaphore_wait(barrier, 3)

    def piece(way, chunk):
        return pl.ds((way * CHUNKS + chunk) * rows, rows)

    def ring_copy(step, way, chunk):
        owner = device(spot - step if way == 0 else spot + step)
        part = piece(way, chunk)
        return pltpu.make_async_remote_copy(
            src_ref=w_ref.at[part] if step == 0 else out_ref.at[owner, part],
            dst_ref=out_ref.at[owner, part],
            send_sem=ring_send.at[step, way, chunk],
            recv_sem=ring_recv.at[step, way, chunk],
            device_id={"sp": ways[way]},
            device_id_type=pl.DeviceIdType.MESH,
        )

    def arrival(step, way, chunk):
        owner = device(spot - step - 1 if way == 0 else spot + step + 1)
        part = piece(way, chunk)
        return pltpu.make_async_remote_copy(
            src_ref=out_ref.at[owner, part],
            dst_ref=out_ref.at[owner, part],
            send_sem=ring_send.at[step, way, chunk],
            recv_sem=ring_recv.at[step, way, chunk],
            device_id={"sp": ways[way]},
            device_id_type=pl.DeviceIdType.MESH,
        )

    def mate_copy(step, way, chunk, incoming=False):
        owner = device(spot - step if way == 0 else spot + step)
        if incoming:
            owner = owner + 1 - 2 * core
        part = piece(way, chunk)
        return pltpu.make_async_remote_copy(
            src_ref=w_ref.at[part] if step == 0 else out_ref.at[owner, part],
            dst_ref=out_ref.at[owner, part],
            send_sem=mate_send.at[step, way, chunk],
            recv_sem=mate_recv.at[step, way, chunk],
            device_id={"sp": mate},
            device_id_type=pl.DeviceIdType.MESH,
        )

    parts = [(way, chunk) for chunk in range(CHUNKS) for way in range(2)]
    for way, chunk in parts:
        ring_copy(0, way, chunk).start()
    for way, chunk in parts:
        mate_copy(0, way, chunk).start()
    own = pltpu.make_async_copy(w_ref, out_ref.at[me], own_sem)
    own.start()
    for step in range(chips - 1):
        for way, chunk in parts:
            arrival(step, way, chunk).wait_recv()
            if step < chips - 2:
                ring_copy(step + 1, way, chunk).start()
            mate_copy(step + 1, way, chunk).start()
    own.wait()
    for step in range(chips):
        for way, chunk in parts:
            if step < chips - 1:
                ring_copy(step, way, chunk).wait_send()
            mate_copy(step, way, chunk).wait_send()
            mate_copy(step, way, chunk, True).wait_recv()


def gather_rows(block):
    n = lax.axis_size("sp")
    chips = n // 2
    rows, cols = block.shape
    return pl.pallas_call(
        functools.partial(ring_kernel, n),
        out_shape=jax.ShapeDtypeStruct((n, rows, cols), block.dtype),
        in_specs=[pl.BlockSpec(memory_space=pltpu.VMEM)],
        out_specs=pl.BlockSpec(memory_space=pl.ANY),
        scratch_shapes=[
            pltpu.SemaphoreType.DMA,
            pltpu.SemaphoreType.DMA((chips - 1, 2, CHUNKS)),
            pltpu.SemaphoreType.DMA((chips - 1, 2, CHUNKS)),
            pltpu.SemaphoreType.DMA((chips, 2, CHUNKS)),
            pltpu.SemaphoreType.DMA((chips, 2, CHUNKS)),
        ],
        compiler_params=pltpu.CompilerParams(
            collective_id=0, has_side_effects=True, vmem_limit_bytes=16 * 2**20
        ),
        cost_estimate=pl.CostEstimate(
            flops=0, bytes_accessed=n * rows * cols * 16, transcendentals=0
        ),
    )(block)


def taps_of(padded, table, length):
    full = padded.shape[0]
    half = table.shape[0] // 2
    total = None
    for k in range(table.shape[0]):
        moved = padded if k == half else pltpu.roll(padded, (half - k) % full, 0)
        term = moved[HALO : HALO + length] * table[k : k + 1].astype(F32)
        total = term if total is None else total + term
    return total


def silu(v):
    return v * jax.nn.sigmoid(v)


def mix_kernel(
    og_ref, ig_ref, va_ref, x_ref, b_ref, c_ref, ct_ref, xt_ref, bt_ref, rt_ref,
    col_ref, row_ref, yconv_ref, within_ref, reads_ref, state_ref,
):
    length = yconv_ref.shape[0]
    gated = (ig_ref[...].astype(F32) * va_ref[...].astype(F32)).astype(BF16).astype(F32)
    conv = taps_of(gated, ct_ref[...], length)
    yconv_ref[...] = (og_ref[pl.ds(HALO, length), :].astype(F32) * conv).astype(BF16)
    xs = silu(taps_of(x_ref[...].astype(F32), xt_ref[...], length)).astype(BF16)
    bs = silu(taps_of(b_ref[...].astype(F32), bt_ref[...], length)).astype(BF16)
    cs = silu(taps_of(c_ref[...].astype(F32), rt_ref[...], length)).astype(BF16)
    reads_ref[...] = cs
    cols = col_ref[0]
    rows = row_ref[0]
    t_at = lax.broadcasted_iota(jnp.int32, (length, length), 0)
    s_at = lax.broadcasted_iota(jnp.int32, (length, length), 1)
    outs, weighted = [], []
    for h in range(2):
        c_h = cs[:, h * STATE : (h + 1) * STATE]
        b_h = bs[:, h * STATE : (h + 1) * STATE]
        x_h = xs[:, h * HEAD_DIM : (h + 1) * HEAD_DIM]
        o = 4 * h
        scores = lax.dot_general(
            c_h, b_h, (((1,), (1,)), ((), ())), preferred_element_type=F32
        )
        gap = jnp.where(
            t_at >= s_at,
            cols[:, o + 2 : o + 3] - rows[o + 2 : o + 3],
            cols[:, o + 3 : o + 4] - rows[o + 3 : o + 4],
        )
        d_f, d_b = rows[o : o + 1], rows[o + 1 : o + 2]
        scale = jnp.where(t_at > s_at, d_f, jnp.where(t_at < s_at, d_b, d_f + d_b))
        w = (scores * jnp.exp(gap) * scale).astype(BF16)
        outs.append(jnp.dot(w, x_h, preferred_element_type=F32))
        x32 = x_h.astype(F32)
        end_f = jnp.exp(rows[o + 2 : o + 3, length - 1 : length] - cols[:, o + 2 : o + 3])
        end_b = jnp.exp(rows[o + 3 : o + 4, 0:1] - cols[:, o + 3 : o + 4])
        both = jnp.concatenate(
            [x32 * (end_f * cols[:, o : o + 1]), x32 * (end_b * cols[:, o + 1 : o + 2])], axis=1
        ).astype(BF16)
        state_ref[h * STATE : (h + 1) * STATE] = lax.dot_general(
            both, b_h, (((0,), (0,)), ((), ())), preferred_element_type=F32
        ).astype(BF16)
    within_ref[...] = jnp.concatenate(outs, axis=1)


def exchange_kernel(
    n, share, s_ref, l_ref, out_ref, got, logs, enter, s_out, s_in, l_out, l_in, e_out, e_in
):
    me = lax.axis_index("sp")
    barrier = pltpu.get_barrier_semaphore()
    for k in range(1, n):
        pl.semaphore_signal(
            barrier,
            inc=1,
            device_id={"sp": (me + k) % n},
            device_id_type=pl.DeviceIdType.MESH,
        )
    pl.semaphore_wait(barrier, n - 1)

    def copy(src, dst, out_sem, in_sem, k, there, slot):
        return pltpu.make_async_remote_copy(
            src_ref=src.at[there],
            dst_ref=dst.at[slot],
            send_sem=out_sem.at[k],
            recv_sem=in_sem.at[k],
            device_id={"sp": there},
            device_id_type=pl.DeviceIdType.MESH,
        )

    for k in range(1, n):
        there = (me + k) % n
        copy(s_ref, got, s_out, s_in, k, there, me).start()
        copy(l_ref, logs, l_out, l_in, k, there, me).start()
    got[me] = s_ref[me]
    logs[me] = l_ref[me]
    for k in range(1, n):
        here = (me + n - k) % n
        copy(s_ref, got, s_out, s_in, k, here, here).wait_recv()
        copy(l_ref, logs, l_out, l_in, k, here, here).wait_recv()
    back = (me * share // HEAD_DIM) % 2
    acc = jnp.zeros(s_ref.shape[1:], F32)
    for i in range(n):
        j = back * (n - 1 - i) + (1 - back) * i
        enter[j] = acc.astype(BF16)
        acc = acc * jnp.exp(logs[j][0:1, :]) + got[j].astype(F32)
    out_ref[me] = enter[me]
    for k in range(1, n):
        copy(enter, out_ref, e_out, e_in, k, (me + k) % n, me).start()
    for k in range(1, n):
        here = (me + n - k) % n
        copy(enter, out_ref, e_out, e_in, k, here, here).wait_recv()
    for k in range(1, n):
        there = (me + k) % n
        copy(s_ref, got, s_out, s_in, k, there, me).wait_send()
        copy(l_ref, logs, l_out, l_in, k, there, me).wait_send()
        copy(enter, out_ref, e_out, e_in, k, there, me).wait_send()


def exchange_states(states, span_log):
    n, share, _ = states.shape
    assert HEAD_DIM % share == 0
    tables = jnp.repeat(span_log.reshape(-1), HEAD_DIM // share)
    tables = jnp.broadcast_to(tables[:, None, None], (n, 8, STATE))
    return pl.pallas_call(
        functools.partial(exchange_kernel, n, share),
        out_shape=jax.ShapeDtypeStruct(states.shape, BF16),
        in_specs=[pl.BlockSpec(memory_space=pltpu.VMEM)] * 2,
        out_specs=pl.BlockSpec(memory_space=pltpu.VMEM),
        scratch_shapes=[
            pltpu.VMEM(states.shape, BF16),
            pltpu.VMEM(tables.shape, F32),
            pltpu.VMEM(states.shape, BF16),
        ]
        + [pltpu.SemaphoreType.DMA((n,))] * 6,
        compiler_params=pltpu.CompilerParams(collective_id=1, has_side_effects=True),
        cost_estimate=pl.CostEstimate(flops=0, bytes_accessed=2**25, transcendentals=0),
    )(states, tables)


def project_kernel(r_ref, w_ref, o_ref):
    o_ref[...] = jnp.dot(r_ref[...], w_ref[...], preferred_element_type=F32).astype(BF16)


def project(rows, weights):
    count, width = rows.shape
    cols = weights.shape[1]
    tile = cols // 9
    return pl.pallas_call(
        project_kernel,
        grid=(9,),
        in_specs=[
            pl.BlockSpec((count, width), lambda j: (0, 0)),
            pl.BlockSpec((width, tile), lambda j: (0, j)),
        ],
        out_specs=pl.BlockSpec((count, tile), lambda j: (0, j)),
        out_shape=jax.ShapeDtypeStruct((count, cols), BF16),
        cost_estimate=pl.CostEstimate(
            flops=2 * count * width * cols, bytes_accessed=2 * width * cols, transcendentals=0
        ),
    )(rows, weights)


def finish_kernel(within_ref, reads_ref, enter_ref, gate_ref, gain_ref, col_ref, y_ref):
    length = y_ref.shape[0]
    cols = col_ref[0]
    outs = []
    for h in range(2):
        o = 4 * h
        both = lax.dot_general(
            reads_ref[:, h * STATE : (h + 1) * STATE],
            enter_ref[h * STATE : (h + 1) * STATE],
            (((1,), (1,)), ((), ())),
            preferred_element_type=F32,
        )
        here = slice(h * HEAD_DIM, (h + 1) * HEAD_DIM)
        y = within_ref[:, here]
        y = y + both[:, :HEAD_DIM] * jnp.exp(cols[:, o + 2 : o + 3])
        y = y + both[:, HEAD_DIM:] * jnp.exp(cols[:, o + 3 : o + 4])
        g = y * silu(gate_ref[pl.ds(HALO, length), :].astype(F32)[:, here])
        g = g * lax.rsqrt(jnp.mean(g * g, axis=-1, keepdims=True) + epsilon)
        outs.append(g * gain_ref[:, here].astype(F32))
    y_ref[...] = jnp.concatenate(outs, axis=1).astype(BF16)


def local(
    layer_source_rows, entry_rescale_factor, sliding_mixer_entry_matrix,
    recurrent_mixer_entry_matrix, latent_write_read_matrix, timestep_matrix,
    sliding_kernel_coefficients, recurrent_kernel_coefficients, latent_kernel_coefficients,
    lane_forgetting_rate, spike_forgetting_rate, lane_rescale_factor,
    sliding_mixer_exit_matrix, recurrent_mixer_exit_matrix,
):
    n = lax.axis_size("sp")
    tp = lax.axis_size("tp")
    own_rows, width = layer_source_rows.shape
    length = own_rows * tp
    full = length + 2 * HALO
    conv_width = sliding_mixer_entry_matrix.shape[2]
    ssd_width = recurrent_mixer_entry_matrix.shape[2]
    state_width = latent_write_read_matrix.shape[2]
    heads = timestep_matrix.shape[2]
    pairs = heads // 2
    cw = conv_width // pairs

    block = jnp.concatenate(
        [sliding_mixer_entry_matrix[i] for i in range(3)]
        + [recurrent_mixer_entry_matrix[i] for i in range(2)]
        + [latent_write_read_matrix[i] for i in range(2)],
        axis=1,
    )
    gathered = gather_rows(block)
    weights = gathered.reshape(n * block.shape[0], block.shape[1])

    x32 = layer_source_rows.astype(F32)
    normed = (
        x32
        * lax.rsqrt(jnp.mean(x32 * x32, axis=-1, keepdims=True) + epsilon)
        * entry_rescale_factor.astype(F32)
    ).astype(BF16)
    up = [(i, i + 1) for i in range(n - 1)]
    down = [(i + 1, i) for i in range(n - 1)]
    before = lax.ppermute(normed[own_rows - HALO :], "sp", up)
    after = lax.ppermute(normed[:HALO], "sp", down)
    shared = lax.all_gather(jnp.concatenate([before, normed, after], axis=0), "tp", axis=0)
    rows = jnp.concatenate(
        [shared[tp - 1, :HALO]]
        + [shared[i, HALO : HALO + own_rows] for i in range(tp)]
        + [shared[0, HALO + own_rows :]],
        axis=0,
    )

    step_weight = timestep_matrix.reshape(width, 2 * heads)
    raw = jnp.dot(rows, step_weight, preferred_element_type=F32).astype(BF16)
    raw = raw[HALO : HALO + length].astype(F32).reshape(length, 2, heads)
    deltas = jax.nn.softplus(raw)
    logs = -deltas * lane_forgetting_rate[None] + spike_forgetting_rate[:, None, :]
    tri = (jnp.arange(length)[:, None] >= jnp.arange(length)[None, :]).astype(F32)
    run_f = jnp.dot(tri, logs[:, 0], precision=HIGHEST)
    run_b = jnp.dot(tri.T, logs[:, 1], precision=HIGHEST)
    table = jnp.stack([deltas[:, 0], deltas[:, 1], run_f, run_b], axis=2)
    col_table = table.reshape(length, pairs, 8).transpose(1, 0, 2)
    row_table = table.reshape(length, pairs, 8).transpose(1, 2, 0)
    span_log = jnp.stack([run_f[length - 1], run_b[0]], axis=1)
    share = heads * 2 * HEAD_DIM // n

    exit_c, exit_s, weights = lax.optimization_barrier(
        (sliding_mixer_exit_matrix, recurrent_mixer_exit_matrix, weights)
    )
    proj = project(rows, weights)
    exit_c = lax.all_gather(exit_c, "sp", axis=1, tiled=True)
    exit_s = lax.all_gather(exit_s, "sp", axis=1, tiled=True)

    latent = latent_kernel_coefficients
    pw, sw = 2 * HEAD_DIM, 2 * STATE
    g0 = 3 * conv_width
    at_gate, at_x = g0 // pw, (g0 + ssd_width) // pw
    at_b = (g0 + 2 * ssd_width) // sw
    at_c = at_b + pairs
    y_conv, within, reads, states = pl.pallas_call(
        mix_kernel,
        grid=(pairs,),
        in_specs=[
            pl.BlockSpec((full, cw), lambda j: (0, j)),
            pl.BlockSpec((full, cw), lambda j: (0, pairs + j)),
            pl.BlockSpec((full, cw), lambda j: (0, 2 * pairs + j)),
            pl.BlockSpec((full, pw), lambda j: (0, at_x + j)),
            pl.BlockSpec((full, sw), lambda j: (0, at_b + j)),
            pl.BlockSpec((full, sw), lambda j: (0, at_c + j)),
            pl.BlockSpec((3, cw), lambda j: (0, j)),
            pl.BlockSpec((5, pw), lambda j: (0, j)),
            pl.BlockSpec((5, sw), lambda j: (0, j)),
            pl.BlockSpec((5, sw), lambda j: (0, pairs + j)),
            pl.BlockSpec((1, length, 8), lambda j: (j, 0, 0)),
            pl.BlockSpec((1, 8, length), lambda j: (j, 0, 0)),
        ],
        out_specs=[
            pl.BlockSpec((length, cw), lambda j: (0, j)),
            pl.BlockSpec((length, pw), lambda j: (0, j)),
            pl.BlockSpec((length, sw), lambda j: (0, j)),
            pl.BlockSpec((sw, STATE), lambda j: (j, 0)),
        ],
        out_shape=[
            jax.ShapeDtypeStruct((length, conv_width), BF16),
            jax.ShapeDtypeStruct((length, ssd_width), F32),
            jax.ShapeDtypeStruct((length, state_width), BF16),
            jax.ShapeDtypeStruct((pairs * sw, STATE), BF16),
        ],
        cost_estimate=pl.CostEstimate(
            flops=8 * length * length * heads * STATE, bytes_accessed=2**24, transcendentals=0
        ),
    )(
        proj, proj, proj, proj, proj, proj,
        sliding_kernel_coefficients, recurrent_kernel_coefficients,
        latent.reshape(latent.shape[0], -1), latent.reshape(latent.shape[0], -1),
        col_table, row_table,
    )

    entering = exchange_states(states.reshape(n, share, STATE), span_log)
    entering = entering.reshape(pairs * sw, STATE)

    y_ssd = pl.pallas_call(
        finish_kernel,
        grid=(pairs,),
        in_specs=[
            pl.BlockSpec((length, pw), lambda j: (0, j)),
            pl.BlockSpec((length, sw), lambda j: (0, j)),
            pl.BlockSpec((sw, STATE), lambda j: (j, 0)),
            pl.BlockSpec((full, pw), lambda j: (0, at_gate + j)),
            pl.BlockSpec((1, pw), lambda j: (0, j)),
            pl.BlockSpec((1, length, 8), lambda j: (j, 0, 0)),
        ],
        out_specs=pl.BlockSpec((length, pw), lambda j: (0, j)),
        out_shape=jax.ShapeDtypeStruct((length, ssd_width), BF16),
    )(within, reads, entering, proj, lane_rescale_factor.reshape(1, -1), col_table)

    def partial(y_c, y_s):
        return (
            jnp.dot(y_c, exit_c, preferred_element_type=F32)
            + jnp.dot(y_s, exit_s, preferred_element_type=F32)
        ).astype(BF16)

    if tp != 2:
        return lax.psum_scatter(
            partial(y_conv, y_ssd), "tp", scatter_dimension=0, tiled=True
        )
    tp_me = lax.axis_index("tp")

    def rows_of(owner, y):
        return lax.dynamic_slice_in_dim(y, owner * own_rows, own_rows, axis=0)

    away = partial(rows_of(1 - tp_me, y_conv), rows_of(1 - tp_me, y_ssd))
    arrived = lax.ppermute(away, "tp", [(0, 1), (1, 0)])
    kept = partial(rows_of(tp_me, y_conv), rows_of(tp_me, y_ssd))
    return (kept.astype(F32) + arrived.astype(F32)).astype(BF16)


def solution(mesh):
    placed = (
        P(("sp", "tp"), None),
        P(),
        P(None, "sp", "tp"),
        P(None, "sp", "tp"),
        P(None, "sp", "tp"),
        P(None, None, "tp"),
        P(None, "tp"),
        P(None, "tp"),
        P(None, None, "tp"),
        P(None, "tp"),
        P("sp", "tp"),
        P("tp"),
        P("tp", "sp"),
        P("tp", "sp"),
    )
    return jax.shard_map(
        local, mesh=mesh, in_specs=placed, out_specs=P(("sp", "tp"), None), check_vma=False
    )
```

profile of v0, /device:TPU:12, one launch (start us, length us, event | category | flops | bytes accessed | tf_op | source)
XLA Modules:
  0.0 236.9 jit_solution(6362669877391688031)
XLA Ops:
  6.5 0.7 convert_element_type.30
  7.3 1.4 fusion.3
  8.6 1.4 fusion.5
  10.1 2.1 collective-permute-start
  12.1 3.8 %collective-permute-start.1 = (bf16[8,2048]{1,0:T(8,128)(2,1)S(1)}, bf16[8,2048]{1,0:T(8,128)(2,1)S(1)}, u32[]{:S(2)}, u32[]{:S(2)}) collective-permute-start(bf16[8,2048]{1,0:T(8,128)(2,1)S(1)} %get-tuple-element.24), channel_id=1, source_target_pairs={{2,0},{4,2},{6,4},{8,6},{10,8},{12,10},{14,12},{16,14},{18,16},{20... | collective-permute-start | bytes 98312 | tf_op jit(solution)/shard_map/ppermute | solution.py:350
  15.9 1.6 collective-permute-done.1
  17.5 1.0 pad_maximum_fusion.1
  18.7 96.4 %shard_map.136 = bf16[16,128,4608]{2,1,0:T(8,128)(2,1)S(1)} custom-call(bf16[128,4608]{1,0:T(8,128)(2,1)S(1)} %bitcast_dynamic-update-slice_fusion.w_ref), custom_call_target="tpu_custom_call" | custom-call | bytes 150994944 | tf_op jit(solution)/shard_map/pallas_call | solution.py:112
  115.1 6.4 %copy-done.1 = bf16[16,128,4608]{2,1,0:T(8,128)(2,1)} copy-done((bf16[16,128,4608]{2,1,0:T(8,128)(2,1)}, bf16[16,128,4608]{2,1,0:T(8,128)(2,1)S(1)}, u32[]{:S(2)}) %copy-start.1) | copy-done | bytes 18874392
  121.7 0.7 all-gather.7.cloned.1.call-update
  122.4 0.6 copy.20
  123.0 0.6 reshape.49.gain_ref
  123.6 0.8 slice_bitcast_fusion.3
  124.4 1.5 slice_bitcast_fusion.1
  126.0 0.5 fusion.16
  126.5 0.2 copy-done.12
  126.9 0.3 fusion.7
  127.2 0.2 fusion.6
  127.5 1.2 copy.18
  128.7 0.2 slice_reduce_fusion.1
  129.1 15.2 %shard_map.137.og_ref.ig_ref.va_ref.x_ref.b_ref.c_ref.gate_ref = bf16[400,4608]{1,0:T(8,128)(2,1)} custom-call(bf16[400,2048]{1,0:T(8,128)(2,1)} %copy-done.4, bf16[2048,4608]{1,0:T(8,128)(2,1)} %bitcast.61), custom_call_target="tpu_custom_call" | custom-call | flops 7549747200 | bytes 18874368 | tf_op jit(solution)/shard_map/pallas_call | solution.py:276
  144.3 10.2 %shard_map.138 = (bf16[384,512]{1,0:T(8,128)(2,1)}, f32[384,512]{1,0:T(8,128)}, bf16[384,1024]{1,0:T(8,128)(2,1)}, bf16[1024,128]{1,0:T(8,128)(2,1)}) custom-call(bf16[400,4608]{1,0:T(8,128)(2,1)} %shard_map.137.og_ref.ig_ref.va_ref.x_ref.b_ref.c_ref.gate_ref, bf16[400,4608]{1,0:T(8,128)(2,1)} %shard_map.137.og_ref.ig_ref.va_ref.x_ref.b_ref.c_ref.gate_ref, ...), custom_call_target="tpu_custom_call" | custom-call | flops 1207959552 | bytes 16777216 | tf_op jit(solution)/shard_map/pallas_call | solution.py:386
  154.5 0.7 broadcast_in_dim.5.l_ref
  155.2 21.0 %shard_map.139 = bf16[16,64,128]{2,1,0:T(8,128)(2,1)} custom-call(bf16[16,64,128]{2,1,0:T(8,128)(2,1)} %bitcast.70, f32[16,8,128]{2,1,0:T(8,128)} %broadcast_in_dim.5.l_ref), custom_call_target="tpu_custom_call" | custom-call | bytes 33554432 | tf_op jit(solution)/shard_map/pallas_call | solution.py:252
  176.2 5.3 %shard_map.140 = bf16[384,512]{1,0:T(8,128)(2,1)} custom-call(f32[384,512]{1,0:T(8,128)} %get-tuple-element.15.within_ref, bf16[384,1024]{1,0:T(8,128)(2,1)} %get-tuple-element.16.reads_ref, bf16[1024,128]{1,0:T(8,128)(2,1)} %bitcast.66, bf16[400,4608]{1,0:T(8,128)(2,1)} %shard_map.137.og_ref.ig_ref.va_ref.x_ref.b_ref.c_ref.gate_ref, ...), custom_call_target="tpu_custom_call" | custom-call | tf_op jit(solution)/shard_map/pallas_call | solution.py:428
  181.5 3.4 %fusion.9 = f32[192,2048]{1,0:T(8,128)} fusion(bf16[512,2048]{1,0:T(8,128)(2,1)} %all-gather.5.cloned.1.call-done, bf16[384,512]{1,0:T(8,128)(2,1)S(1)} %copy-done.8, s32[]{:T(128)S(6)} %select_n.14), kind=kOutput, calls=%fused_computation.21 | convolution fusion | flops 402653184 | bytes 3866628 | tf_op jit(solution)/shard_map/dot_general | solution.py:445
  184.9 20.3 %all-gather.7.cloned.1.call-done = bf16[512,2048]{1,0:T(8,128)(2,1)} async-done(((bf16[512,128]{1,0:T(8,128)(2,1)}), bf16[512,2048]{1,0:T(8,128)(2,1)}) %all-gather.7.cloned.1.call-update) | async-done | bytes 2097168 | tf_op jit(solution)/shard_map/all_gather | solution.py:378
  205.2 2.6 %fusion.2 = bf16[192,2048]{1,0:T(8,128)(2,1)S(1)} fusion(f32[192,2048]{1,0:T(8,128)} %fusion.9, bf16[512,2048]{1,0:T(8,128)(2,1)} %all-gather.7.cloned.1.call-done, bf16[384,512]{1,0:T(8,128)(2,1)S(1)} %copy-done.5, s32[]{:T(128)S(6)} %select_n.14), kind=kOutput, calls=%fused_computation.4 | convolution fusion | flops 403439616 | bytes 4653060 | tf_op jit(solution)/shard_map/dot_general | solution.py:446
  207.9 1.5 collective-permute-start.2
  209.4 1.7 fusion.14
  211.1 16.7 %collective-permute-done.2 = bf16[192,2048]{1,0:T(8,128)(2,1)} collective-permute-done((bf16[192,2048]{1,0:T(8,128)(2,1)S(1)}, bf16[192,2048]{1,0:T(8,128)(2,1)}, u32[]{:S(2)}, u32[]{:S(2)}) %collective-permute-start.2) | collective-permute-done | bytes 786464 | tf_op jit(solution)/shard_map/ppermute | solution.py:459
  227.7 2.6 %add_convert_fusion = bf16[192,2048]{1,0:T(8,128)(2,1)} fusion(bf16[192,2048]{1,0:T(8,128)(2,1)} %collective-permute-done.2, f32[192,2048]{1,0:T(8,128)S(1)} %fusion.14, bf16[512,2048]{1,0:T(8,128)(2,1)S(1)} %copy-done.2, bf16[384,512]{1,0:T(8,128)(2,1)S(1)} %copy-done.5, s32[]{:T(128)S(6)} %select_n.13), kind=kOutput, calls=%fused_computation.11 | convolution fusion | flops 405012480 | bytes 5439492 | tf_op jit(solution)/shard_map/dot_general | solution.py:446
  (55 shorter events, 0.9 us)
Async XLA Ops:
  6.5 119.4 %copy-start = (bf16[2048,2,8]{0,2,1:T(8,128)(2,1)S(1)}, bf16[2048,2,8]{0,2,1:T(8,128)(2,1)}, u32[]{:S(2)}) copy-start(bf16[2048,2,8]{0,2,1:T(8,128)(2,1)} %param.19) | copy-start | bytes 196612
  6.5 117.1 %all-gather.9.cloned.1.call-start = ((), (), s32[]{:S(2)}) async-start(), calls=%async_computation.2 | async-start | bytes 2555904 | tf_op jit(solution)/shard_map/all_gather | solution.py:351
  10.0 8.5 %copy-start.9 = (bf16[3,128,512]{2,1,0:T(8,128)(2,1)S(1)}, bf16[3,128,512]{2,1,0:T(8,128)(2,1)}, u32[]{:S(2)}) copy-start(bf16[3,128,512]{2,1,0:T(8,128)(2,1)} %param.16) | copy-start | bytes 1179652
  10.1 5.9 %collective-permute-start = (bf16[8,2048]{1,0:T(8,128)(2,1)S(1)}, bf16[8,2048]{1,0:T(8,128)(2,1)S(1)}, u32[]{:S(2)}, u32[]{:S(2)}) collective-permute-start(bf16[8,2048]{1,0:T(8,128)(2,1)S(1)} %get-tuple-element.23), channel_id=1, source_target_pairs={{0,2},{2,4},{4,6},{6,8},{8,10},{10,12},{12,14},{14,16},{16,18},{18... | collective-permute-start | bytes 98312 | tf_op jit(solution)/shard_map/ppermute | solution.py:349
  12.1 6.5 %copy-start.10 = (bf16[2,128,512]{2,1,0:T(8,128)(2,1)S(1)}, bf16[2,128,512]{2,1,0:T(8,128)(2,1)}, u32[]{:S(2)}) copy-start(bf16[2,128,512]{2,1,0:T(8,128)(2,1)} %param.17) | copy-start | bytes 786436
  12.1 6.5 %copy-start.6 = (bf16[2,128,1024]{2,1,0:T(8,128)(2,1)S(1)}, bf16[2,128,1024]{2,1,0:T(8,128)(2,1)}, u32[]{:S(2)}) copy-start(bf16[2,128,1024]{2,1,0:T(8,128)(2,1)} %param.18) | copy-start | bytes 1572868
  12.1 5.4 %collective-permute-start.1 = (bf16[8,2048]{1,0:T(8,128)(2,1)S(1)}, bf16[8,2048]{1,0:T(8,128)(2,1)S(1)}, u32[]{:S(2)}, u32[]{:S(2)}) collective-permute-start(bf16[8,2048]{1,0:T(8,128)(2,1)S(1)} %get-tuple-element.24), channel_id=1, source_target_pairs={{2,0},{4,2},{6,4},{8,6},{10,8},{12,10},{14,12},{16,14},{18,16},{20... | collective-permute-start | bytes 98312 | tf_op jit(solution)/shard_map/ppermute | solution.py:350
  18.5 163.0 %all-gather.5.cloned.1.call-start = ((), (), s32[]{:S(2)}) async-start(), calls=%async_computation | async-start | bytes 2228224 | tf_op jit(solution)/shard_map/all_gather | solution.py:377
  18.7 103.7 %copy-start.11 = (bf16[5,2,1024]{2,1,0:T(2,128)(2,1)S(1)}, bf16[5,2,1024]{2,1,0:T(2,128)(2,1)}, u32[]{:S(2)}) copy-start(bf16[5,2,1024]{2,1,0:T(2,128)(2,1)} %param.22) | copy-start | bytes 61444
  18.7 104.3 %copy-start.14 = (bf16[512]{0:T(512)(128)(2,1)S(1)}, bf16[512]{0:T(512)(128)(2,1)}, u32[]{:S(2)}) copy-start(bf16[512]{0:T(512)(128)(2,1)} %param.25) | copy-start | bytes 3076
  115.1 6.5 %copy-start.1 = (bf16[16,128,4608]{2,1,0:T(8,128)(2,1)}, bf16[16,128,4608]{2,1,0:T(8,128)(2,1)S(1)}, u32[]{:S(2)}) copy-start(bf16[16,128,4608]{2,1,0:T(8,128)(2,1)S(1)} %shard_map.136) | copy-start | bytes 56623108
  121.6 83.6 %all-gather.7.cloned.1.call-start = ((), (), s32[]{:S(2)}) async-start(), calls=%async_computation.1 | async-start | bytes 2228224 | tf_op jit(solution)/shard_map/all_gather | solution.py:378
  126.0 2.7 %copy-start.4 = (bf16[400,2048]{1,0:T(8,128)(2,1)}, bf16[400,2048]{1,0:T(8,128)(2,1)S(1)}, u32[]{:S(2)}) copy-start(bf16[400,2048]{1,0:T(8,128)(2,1)S(1)} %pad_maximum_fusion.r_ref) | copy-start | bytes 4915204
  126.0 0.7 copy-start.12
  126.0 0.8 copy-start.13
  127.5 16.8 %copy-start.7 = (f32[384,4,8]{0,2,1:T(8,128)}, f32[384,4,8]{0,2,1:T(8,128)S(1)}, u32[]{:S(2)}) copy-start(f32[384,4,8]{0,2,1:T(8,128)S(1)} %reshape.46) | copy-start | bytes 147460
  176.2 5.3 %copy-start.8 = (bf16[384,512]{1,0:T(8,128)(2,1)S(1)}, bf16[384,512]{1,0:T(8,128)(2,1)}, u32[]{:S(2)}) copy-start(bf16[384,512]{1,0:T(8,128)(2,1)} %get-tuple-element.13) | copy-start | bytes 1179652
  181.5 23.7 %copy-start.5 = (bf16[384,512]{1,0:T(8,128)(2,1)S(1)}, bf16[384,512]{1,0:T(8,128)(2,1)}, u32[]{:S(2)}) copy-start(bf16[384,512]{1,0:T(8,128)(2,1)} %shard_map.140) | copy-start | bytes 1179652
  184.9 24.5 %copy-start.3 = (bf16[512,2048]{1,0:T(8,128)(2,1)S(1)}, bf16[512,2048]{1,0:T(8,128)(2,1)}, u32[]{:S(2)}) copy-start(bf16[512,2048]{1,0:T(8,128)(2,1)} %all-gather.5.cloned.1.call-done) | copy-start | bytes 6291460
  207.9 19.9 %collective-permute-start.2 = (bf16[192,2048]{1,0:T(8,128)(2,1)S(1)}, bf16[192,2048]{1,0:T(8,128)(2,1)}, u32[]{:S(2)}, u32[]{:S(2)}) collective-permute-start(bf16[192,2048]{1,0:T(8,128)(2,1)S(1)} %fusion.2), channel_id=1, source_target_pairs={{0,1},{1,0},{2,3},{3,2},{4,5},{5,4},{6,7},{7,6},{8,9},{9,8},{10,11... | collective-permute-start | bytes 2359304 | tf_op jit(solution)/shard_map/ppermute | solution.py:459
  209.4 18.3 %copy-start.2 = (bf16[512,2048]{1,0:T(8,128)(2,1)S(1)}, bf16[512,2048]{1,0:T(8,128)(2,1)}, u32[]{:S(2)}) copy-start(bf16[512,2048]{1,0:T(8,128)(2,1)} %all-gather.7.cloned.1.call-done) | copy-start | bytes 6291460
Sparse Core Ops, SparseCore 0:
  18.6 30.9 all-gather.8
  121.7 40.4 all-gather.4
  164.4 40.8 all-gather.6
where the time goes:
time: 240 us; the launch traced here: 237 us
  Pallas kernels  148 us (62%)
  waiting for transfers between devices  39.3 us (16%)
  between operations  13.4 us (6%)
  local copies, waits for them, and re-layouts  12.7 us (5%)
  matrix products  11.3 us (5%)
  starting transfers between devices  7.44 us (3%)
  other arithmetic  4.66 us (2%)
    pallas_call x1, Pallas kernels, gather_rows(): pl.pallas_call(functools.partial(ring_kernel, n), out_shape=jax.ShapeDtyp...  96.4 us
    pallas_call x1, Pallas kernels, exchange_states(): pl.pallas_call(functools.partial(exchange_kernel, n, share), out_shape=ja...  21 us
    all_gather x1, waiting for transfers between devices, local(): exit_s = lax.all_gather(exit_s, 'sp', axis=1, tiled=True)  20.3 us
    ppermute x1, waiting for transfers between devices, local(): arrived = lax.ppermute(away, 'tp', [(0, 1), (1, 0)])  16.7 us
    pallas_call x1, Pallas kernels, project(): pl.pallas_call(project_kernel, grid=(9,), in_specs=[pl.BlockSpec((count,...  15.2 us
    pallas_call x1, Pallas kernels, local(): pl.pallas_call(mix_kernel, grid=(pairs,), in_specs=[pl.BlockSpec((full, c...  10.2 us
    unnamed x37, local copies, waits for them, and re-layouts  7.44 us
    pallas_call x1, Pallas kernels, local(): pl.pallas_call(finish_kernel, grid=(pairs,), in_specs=[pl.BlockSpec((leng...  5.27 us
  transfers between devices with their start and end apart: 6, of which 3 were waited for; matrix products, arithmetic and copies ran while one was open for 5% of the time, Pallas kernels for 62%

commit v1 on v0

--- a/solution.py
+++ b/solution.py
@@ -9,7 +9,7 @@
 
 HEAD_DIM = 64
 STATE = 128
-HALO = 8
+HALO = 16
 CHUNKS = 2
 epsilon = 1e-05
 F32 = jnp.float32
@@ -265,6 +265,467 @@
     )(states, tables)
 
 
+def ring_spot(n):
+    chips = n // 2
+    me = lax.axis_index("sp")
+    core, chip = me % 2, me // 2
+    odd = chip % 2
+    spot = (1 - odd) * (chip // 2) + odd * (chips - 1 - chip // 2)
+
+    def device(position):
+        position = (position + 2 * chips) % chips
+        half = (chips + 1) // 2
+        late = position // half
+        late_chip = 2 * (chips - 1 - position) + 1
+        return 2 * ((1 - late) * 2 * position + late * late_chip) + core
+
+    return me, core, spot, device
+
+
+def send_to(src, dst, out_sem, in_sem, target):
+    return pltpu.make_async_remote_copy(
+        src_ref=src,
+        dst_ref=dst,
+        send_sem=out_sem,
+        recv_sem=in_sem,
+        device_id=target,
+        device_id_type=pl.DeviceIdType.MESH,
+    )
+
+
+def softplus(v):
+    return jnp.maximum(v, 0.0) + jnp.log1p(jnp.exp(-jnp.abs(v)))
+
+
+def front_kernel(
+    n, x_ref, gain_ref, conv_ref, rec_ref, lat_ref, step_ref, rate_ref, spike_ref,
+    proj_ref, table_ref,
+    w_buf, raw, normed, acc, own_sems, x_own, x_send, x_recv,
+    ring_send, ring_recv, mate_send, mate_recv,
+):
+    chips = n // 2
+    me, core, spot, device = ring_spot(n)
+    tp_me = lax.axis_index("tp")
+    mate = me + 1 - 2 * core
+    ways = (device(spot + 1), device(spot - 1))
+    own_rows, width = x_ref.shape
+    depth = w_buf.shape[0] // n
+    length = 2 * own_rows
+    piece = w_buf.shape[1] // (2 * CHUNKS)
+
+    offset, own = 0, []
+    for ref in (conv_ref, rec_ref, lat_ref):
+        for i in range(ref.shape[0]):
+            cols = ref.shape[2]
+            own.append(
+                pltpu.make_async_copy(
+                    ref.at[i],
+                    w_buf.at[pl.ds(pl.multiple_of(me * depth, depth), depth), pl.ds(offset, cols)],
+                    own_sems.at[len(own)],
+                )
+            )
+            offset += cols
+    for copy in own:
+        copy.start()
+
+    up, down = (me + 1) % n, (me + n - 1) % n
+    barrier = pltpu.get_barrier_semaphore()
+    greeted = [{"sp": other} for other in (mate,) + ways] + [{"tp": 1 - tp_me}]
+    greeted += [{"sp": other, "tp": t} for other in (up, down) for t in range(2)]
+    for other in greeted:
+        pl.semaphore_signal(
+            barrier, inc=1, device_id=other, device_id_type=pl.DeviceIdType.MESH
+        )
+    pl.semaphore_wait(barrier, len(greeted))
+
+    def rows_of(owner):
+        return pl.ds(pl.multiple_of(owner * depth, depth), depth)
+
+    def cols_of(way, chunk):
+        return pl.ds((way * CHUNKS + chunk) * piece, piece)
+
+    def owner_of(step, way):
+        return device(spot - step if way == 0 else spot + step)
+
+    def ring_copy(step, way, chunk, shift=0):
+        part = w_buf.at[rows_of(owner_of(step + shift, way)), cols_of(way, chunk)]
+        at = (step, way, chunk)
+        return send_to(part, part, ring_send.at[at], ring_recv.at[at], {"sp": ways[way]})
+
+    def mate_copy(step, way, chunk, incoming=False):
+        owner = owner_of(step, way)
+        if incoming:
+            owner = owner + 1 - 2 * core
+        part = w_buf.at[rows_of(owner), cols_of(way, chunk)]
+        at = (step, way, chunk)
+        return send_to(part, part, mate_send.at[at], mate_recv.at[at], {"sp": mate})
+
+    parts = [(way, chunk) for chunk in range(CHUNKS) for way in range(2)]
+    for copy in own:
+        copy.wait()
+    for way, chunk in parts:
+        ring_copy(0, way, chunk).start()
+    for way, chunk in parts:
+        mate_copy(0, way, chunk).start()
+
+    mine = pl.ds(pl.multiple_of(HALO + own_rows * tp_me, HALO), own_rows)
+    across = send_to(x_ref, raw.at[mine], x_send.at[0], x_recv.at[0], {"tp": 1 - tp_me})
+    across.start()
+    here = pltpu.make_async_copy(x_ref, raw.at[mine], x_own)
+    here.start()
+    before, after = pl.ds(0, HALO), pl.ds(HALO + length, HALO)
+
+    def halo(t, low):
+        if low:
+            return send_to(
+                x_ref.at[pl.ds(own_rows - HALO, HALO)], raw.at[before],
+                x_send.at[1 + t], x_recv.at[1], {"sp": up, "tp": t},
+            )
+        return send_to(
+            x_ref.at[pl.ds(0, HALO)], raw.at[after],
+            x_send.at[1 + t], x_recv.at[2], {"sp": down, "tp": t},
+        )
+
+    sends_up = jnp.logical_and(tp_me == 1, me < n - 1)
+    sends_down = jnp.logical_and(tp_me == 0, me > 0)
+
+    @pl.when(sends_up)
+    def _():
+        for t in range(2):
+            halo(t, True).start()
+
+    @pl.when(sends_down)
+    def _():
+        for t in range(2):
+            halo(t, False).start()
+
+    @pl.when(me == 0)
+    def _():
+        raw[0:HALO, :] = jnp.zeros((HALO, width), BF16)
+
+    @pl.when(me == n - 1)
+    def _():
+        raw[HALO + length :, :] = jnp.zeros((HALO, width), BF16)
+
+    here.wait()
+    across.wait()
+
+    @pl.when(me > 0)
+    def _():
+        halo(0, True).wait_recv()
+
+    @pl.when(me < n - 1)
+    def _():
+        halo(0, False).wait_recv()
+
+    @pl.when(sends_up)
+    def _():
+        for t in range(2):
+            halo(t, True).wait_send()
+
+    @pl.when(sends_down)
+    def _():
+        for t in range(2):
+            halo(t, False).wait_send()
+
+    gain = gain_ref[...].astype(F32)
+    tall = 2 * HALO
+
+    def norm_block(i, _):
+        at = pl.ds(pl.multiple_of(i * tall, tall), tall)
+        x32 = raw[at, :].astype(F32)
+        scale = lax.rsqrt(jnp.mean(x32 * x32, axis=-1, keepdims=True) + epsilon)
+        normed[at, :] = (x32 * scale * gain).astype(BF16)
+        return 0
+
+    lax.fori_loop(0, raw.shape[0] // tall, norm_block, 0)
+
+    def dot_part(step, way, chunk, first=False):
+        start = pl.multiple_of((owner_of(step, way) - core) * depth, 2 * depth)
+        span = pl.ds(start, 2 * depth)
+        cols = cols_of(way, chunk)
+        value = jnp.dot(normed[:, span], w_buf[span, cols], preferred_element_type=F32)
+        if first:
+            acc[:, cols] = value
+        else:
+            acc[:, cols] += value
+
+    def forward(step, way, chunk):
+        ring_copy(step, way, chunk, 1).wait_recv()
+
+        @pl.when(step < chips - 2)
+        def _():
+            ring_copy(step + 1, way, chunk).start()
+
+        mate_copy(step + 1, way, chunk).start()
+
+    for way, chunk in parts:
+        forward(0, way, chunk)
+    for way, chunk in parts:
+        mate_copy(0, way, chunk, True).wait_recv()
+        dot_part(0, way, chunk, True)
+
+    heads = spike_ref.shape[1]
+    raw_step = jnp.dot(
+        normed[HALO : HALO + length, :], step_ref[...], preferred_element_type=F32
+    ).astype(BF16)
+    row = lax.broadcasted_iota(jnp.int32, (2 * heads, 4 * heads), 0)
+    col = lax.broadcasted_iota(jnp.int32, (2 * heads, 4 * heads), 1)
+    pick = jnp.where((row % heads == col // 4) & (row // heads == col % 2), 1.0, 0.0)
+    head_row = lax.broadcasted_iota(jnp.int32, (heads, 4 * heads), 0)
+    head_col = lax.broadcasted_iota(jnp.int32, (heads, 4 * heads), 1)
+    spread = jnp.where(head_row == head_col // 4, 1.0, 0.0).astype(F32)
+    deltas = softplus(jnp.dot(raw_step, pick.astype(BF16), preferred_element_type=F32))
+    rates = jnp.dot(rate_ref[...], spread, precision=HIGHEST, preferred_element_type=F32)
+    side = lax.broadcasted_iota(jnp.int32, (2, 4 * heads), 0)
+    kind2 = lax.broadcasted_iota(jnp.int32, (2, 4 * heads), 1) % 2
+    rates = jnp.sum(jnp.where(side == kind2, rates, 0.0), axis=0, keepdims=True)
+    spikes = jnp.dot(spike_ref[...], spread, precision=HIGHEST, preferred_element_type=F32)
+    logs = spikes - deltas * rates
+    t_at = lax.broadcasted_iota(jnp.int32, (length, length), 0)
+    s_at = lax.broadcasted_iota(jnp.int32, (length, length), 1)
+    tri = jnp.where(t_at >= s_at, 1.0, 0.0).astype(F32)
+    run_f = jnp.dot(tri, logs, precision=HIGHEST, preferred_element_type=F32)
+    tri = jnp.where(t_at <= s_at, 1.0, 0.0).astype(F32)
+    run_b = jnp.dot(tri, logs, precision=HIGHEST, preferred_element_type=F32)
+    kind = lax.broadcasted_iota(jnp.int32, (length, 4 * heads), 1) % 4
+    table_ref[...] = jnp.where(kind < 2, deltas, jnp.where(kind == 2, run_f, run_b))
+
+    def ring_step(step, _):
+        for way, chunk in parts:
+            forward(step, way, chunk)
+            mate_copy(step, way, chunk, True).wait_recv()
+            dot_part(step, way, chunk)
+        return 0
+
+    lax.fori_loop(1, chips - 1, ring_step, 0)
+    for way, chunk in parts:
+        mate_copy(chips - 1, way, chunk, True).wait_recv()
+        dot_part(chips - 1, way, chunk)
+        cols = cols_of(way, chunk)
+        proj_ref[:, cols] = acc[:, cols].astype(BF16)
+
+    def drain(step, _):
+        for way, chunk in parts:
+            @pl.when(step < chips - 1)
+            def _():
+                ring_copy(step, way, chunk).wait_send()
+
+            mate_copy(step, way, chunk).wait_send()
+        return 0
+
+    lax.fori_loop(0, chips, drain, 0)
+
+
+def front(rows, gain, conv_w, rec_w, lat_w, step_w, rate, spike):
+    n = lax.axis_size("sp")
+    chips = n // 2
+    own_rows, width = rows.shape
+    length = 2 * own_rows
+    full = length + 2 * HALO
+    depth = conv_w.shape[1]
+    cols = sum(w.shape[0] * w.shape[2] for w in (conv_w, rec_w, lat_w))
+    blocks = sum(w.shape[0] for w in (conv_w, rec_w, lat_w))
+    heads = spike.shape[1]
+    vmem = pl.BlockSpec(memory_space=pltpu.VMEM)
+    hbm = pl.BlockSpec(memory_space=pl.ANY)
+    return pl.pallas_call(
+        functools.partial(front_kernel, n),
+        out_shape=[
+            jax.ShapeDtypeStruct((full, cols), BF16),
+            jax.ShapeDtypeStruct((length, 4 * heads), F32),
+        ],
+        in_specs=[vmem, vmem, hbm, hbm, hbm, vmem, vmem, vmem],
+        out_specs=[vmem, vmem],
+        scratch_shapes=[
+            pltpu.VMEM((n * depth, cols), BF16),
+            pltpu.VMEM((full, width), BF16),
+            pltpu.VMEM((full, width), BF16),
+            pltpu.VMEM((full, cols), F32),
+            pltpu.SemaphoreType.DMA((blocks,)),
+            pltpu.SemaphoreType.DMA,
+            pltpu.SemaphoreType.DMA((3,)),
+            pltpu.SemaphoreType.DMA((3,)),
+            pltpu.SemaphoreType.DMA((chips - 1, 2, CHUNKS)),
+            pltpu.SemaphoreType.DMA((chips - 1, 2, CHUNKS)),
+            pltpu.SemaphoreType.DMA((chips, 2, CHUNKS)),
+            pltpu.SemaphoreType.DMA((chips, 2, CHUNKS)),
+        ],
+        compiler_params=pltpu.CompilerParams(
+            collective_id=2, has_side_effects=True, vmem_limit_bytes=56 * 2**20
+        ),
+        cost_estimate=pl.CostEstimate(
+            flops=2 * full * width * cols, bytes_accessed=2 * width * cols, transcendentals=0
+        ),
+    )(rows, gain.reshape(1, -1), conv_w, rec_w, lat_w, step_w, rate, spike)
+
+
+def exit_ring(n, c_ref, s_ref, c_out, s_out, own_sems, sems):
+    chips = n // 2
+    me, core, spot, device = ring_spot(n)
+    mate = me + 1 - 2 * core
+    ways = (device(spot + 1), device(spot - 1))
+    ring_send, ring_recv, mate_send, mate_recv = sems
+    refs, outs = (c_ref, s_ref), (c_out, s_out)
+    rows, wide = c_ref.shape
+    tall = rows // CHUNKS
+
+    def spot_in(owner, way, chunk):
+        cols = pl.ds(pl.multiple_of(owner * wide, wide), wide)
+        return outs[way].at[pl.ds(chunk * tall, tall), cols]
+
+    def owner_of(step, way):
+        return device(spot - step if way == 0 else spot + step)
+
+    def source(step, way, chunk):
+        if step == 0:
+            return refs[way].at[pl.ds(chunk * tall, tall)]
+        return spot_in(owner_of(step, way), way, chunk)
+
+    def ring_copy(step, way, chunk):
+        at = (step, way, chunk)
+        return send_to(
+            source(step, way, chunk), spot_in(owner_of(step, way), way, chunk),
+            ring_send.at[at], ring_recv.at[at], {"sp": ways[way]},
+        )
+
+    def arrival(step, way, chunk):
+        part = spot_in(owner_of(step + 1, way), way, chunk)
+        at = (step, way, chunk)
+        return send_to(part, part, ring_send.at[at], ring_recv.at[at], {"sp": ways[way]})
+
+    def mate_copy(step, way, chunk, incoming=False):
+        owner = owner_of(step, way)
+        at = (step, way, chunk)
+        there = spot_in(owner + 1 - 2 * core if incoming else owner, way, chunk)
+        src = there if incoming else source(step, way, chunk)
+        return send_to(src, there, mate_send.at[at], mate_recv.at[at], {"sp": mate})
+
+    parts = [(way, chunk) for chunk in range(CHUNKS) for way in range(2)]
+    cols = pl.ds(pl.multiple_of(me * wide, wide), wide)
+    own = [
+        pltpu.make_async_copy(refs[way], outs[way].at[:, cols], own_sems.at[way])
+        for way in range(2)
+    ]
+
+    def start():
+        for way, chunk in parts:
+            ring_copy(0, way, chunk).start()
+        for way, chunk in parts:
+            mate_copy(0, way, chunk).start()
+        for copy in own:
+            copy.start()
+
+    def advance(step):
+        for way, chunk in parts:
+            arrival(step, way, chunk).wait_recv()
+            if step < chips - 2:
+                ring_copy(step + 1, way, chunk).start()
+            mate_copy(step + 1, way, chunk).start()
+
+    def finish():
+        for copy in own:
+            copy.wait()
+        for step in range(chips):
+            for way, chunk in parts:
+                if step < chips - 1:
+                    ring_copy(step, way, chunk).wait_send()
+                mate_copy(step, way, chunk).wait_send()
+                mate_copy(step, way, chunk, True).wait_recv()
+
+    return chips, start, advance, finish
+
+
+def exchange_exit_kernel(
+    n, share, s_ref, l_ref, c_ref, x_ref, out_ref, c_out, x_out,
+    got, logs, enter, s_sem, s_in, l_out, l_in, e_out, e_in,
+    own_sems, ring_send, ring_recv, mate_send, mate_recv,
+):
+    me = lax.axis_index("sp")
+    barrier = pltpu.get_barrier_semaphore()
+    for k in range(1, n):
+        pl.semaphore_signal(
+            barrier,
+            inc=1,
+            device_id={"sp": (me + k) % n},
+            device_id_type=pl.DeviceIdType.MESH,
+        )
+    pl.semaphore_wait(barrier, n - 1)
+    chips, start, advance, finish = exit_ring(
+        n, c_ref, x_ref, c_out, x_out, own_sems, (ring_send, ring_recv, mate_send, mate_recv)
+    )
+
+    def copy(src, dst, out_sem, in_sem, k, there, slot):
+        return send_to(
+            src.at[there], dst.at[slot], out_sem.at[k], in_sem.at[k], {"sp": there}
+        )
+
+    for k in range(1, n):
+        there = (me + k) % n
+        copy(s_ref, got, s_sem, s_in, k, there, me).start()
+        copy(l_ref, logs, l_out, l_in, k, there, me).start()
+    start()
+    got[me] = s_ref[me]
+    logs[me] = l_ref[me]
+    advance(0)
+    advance(1)
+    for k in range(1, n):
+        here = (me + n - k) % n
+        copy(s_ref, got, s_sem, s_in, k, here, here).wait_recv()
+        copy(l_ref, logs, l_out, l_in, k, here, here).wait_recv()
+    back = (me * share // HEAD_DIM) % 2
+    acc = jnp.zeros(s_ref.shape[1:], F32)
+    for i in range(n):
+        j = back * (n - 1 - i) + (1 - back) * i
+        enter[j] = acc.astype(BF16)
+        acc = acc * jnp.exp(logs[j][0:1, :]) + got[j].astype(F32)
+    out_ref[me] = enter[me]
+    for k in range(1, n):
+        copy(enter, out_ref, e_out, e_in, k, (me + k) % n, me).start()
+    for step in range(2, chips - 1):
+        advance(step)
+    for k in range(1, n):
+        here = (me + n - k) % n
+        copy(enter, out_ref, e_out, e_in, k, here, here).wait_recv()
+    for k in range(1, n):
+        there = (me + k) % n
+        copy(s_ref, got, s_sem, s_in, k, there, me).wait_send()
+        copy(l_ref, logs, l_out, l_in, k, there, me).wait_send()
+        copy(enter, out_ref, e_out, e_in, k, there, me).wait_send()
+    finish()
+
+
+def exchange_exit(states, span_log, exit_c, exit_s):
+    n, share, _ = states.shape
+    chips = n // 2
+    assert HEAD_DIM % share == 0
+    tables = jnp.repeat(span_log.reshape(-1), HEAD_DIM // share)
+    tables = jnp.broadcast_to(tables[:, None, None], (n, 8, STATE))
+    wide = (exit_c.shape[0], exit_c.shape[1] * n)
+    vmem = pl.BlockSpec(memory_space=pltpu.VMEM)
+    return pl.pallas_call(
+        functools.partial(exchange_exit_kernel, n, share),
+        out_shape=[
+            jax.ShapeDtypeStruct(states.shape, BF16),
+            jax.ShapeDtypeStruct(wide, BF16),
+            jax.ShapeDtypeStruct(wide, BF16),
+        ],
+        in_specs=[vmem] * 4,
+        out_specs=[vmem] * 3,
+        scratch_shapes=[
+            pltpu.VMEM(states.shape, BF16),
+            pltpu.VMEM(tables.shape, F32),
+            pltpu.VMEM(states.shape, BF16),
+        ]
+        + [pltpu.SemaphoreType.DMA((n,))] * 6
+        + [pltpu.SemaphoreType.DMA((2,))]
+        + [pltpu.SemaphoreType.DMA((chips - 1, 2, CHUNKS))] * 2
+        + [pltpu.SemaphoreType.DMA((chips, 2, CHUNKS))] * 2,
+        compiler_params=pltpu.CompilerParams(collective_id=3, has_side_effects=True),
+        cost_estimate=pl.CostEstimate(flops=0, bytes_accessed=2**25, transcendentals=0),
+    )(states, tables, exit_c, exit_s)
+
+
 def project_kernel(r_ref, w_ref, o_ref):
     o_ref[...] = jnp.dot(r_ref[...], w_ref[...], preferred_element_type=F32).astype(BF16)
 
@@ -329,53 +790,65 @@
     pairs = heads // 2
     cw = conv_width // pairs
 
-    block = jnp.concatenate(
-        [sliding_mixer_entry_matrix[i] for i in range(3)]
-        + [recurrent_mixer_entry_matrix[i] for i in range(2)]
-        + [latent_write_read_matrix[i] for i in range(2)],
-        axis=1,
-    )
-    gathered = gather_rows(block)
-    weights = gathered.reshape(n * block.shape[0], block.shape[1])
-
-    x32 = layer_source_rows.astype(F32)
-    normed = (
-        x32
-        * lax.rsqrt(jnp.mean(x32 * x32, axis=-1, keepdims=True) + epsilon)
-        * entry_rescale_factor.astype(F32)
-    ).astype(BF16)
-    up = [(i, i + 1) for i in range(n - 1)]
-    down = [(i + 1, i) for i in range(n - 1)]
-    before = lax.ppermute(normed[own_rows - HALO :], "sp", up)
-    after = lax.ppermute(normed[:HALO], "sp", down)
-    shared = lax.all_gather(jnp.concatenate([before, normed, after], axis=0), "tp", axis=0)
-    rows = jnp.concatenate(
-        [shared[tp - 1, :HALO]]
-        + [shared[i, HALO : HALO + own_rows] for i in range(tp)]
-        + [shared[0, HALO + own_rows :]],
-        axis=0,
-    )
-
-    step_weight = timestep_matrix.reshape(width, 2 * heads)
-    raw = jnp.dot(rows, step_weight, preferred_element_type=F32).astype(BF16)
-    raw = raw[HALO : HALO + length].astype(F32).reshape(length, 2, heads)
-    deltas = jax.nn.softplus(raw)
-    logs = -deltas * lane_forgetting_rate[None] + spike_forgetting_rate[:, None, :]
-    tri = (jnp.arange(length)[:, None] >= jnp.arange(length)[None, :]).astype(F32)
-    run_f = jnp.dot(tri, logs[:, 0], precision=HIGHEST)
-    run_b = jnp.dot(tri.T, logs[:, 1], precision=HIGHEST)
-    table = jnp.stack([deltas[:, 0], deltas[:, 1], run_f, run_b], axis=2)
-    col_table = table.reshape(length, pairs, 8).transpose(1, 0, 2)
-    row_table = table.reshape(length, pairs, 8).transpose(1, 2, 0)
-    span_log = jnp.stack([run_f[length - 1], run_b[0]], axis=1)
     share = heads * 2 * HEAD_DIM // n
-
-    exit_c, exit_s, weights = lax.optimization_barrier(
-        (sliding_mixer_exit_matrix, recurrent_mixer_exit_matrix, weights)
-    )
-    proj = project(rows, weights)
-    exit_c = lax.all_gather(exit_c, "sp", axis=1, tiled=True)
-    exit_s = lax.all_gather(exit_s, "sp", axis=1, tiled=True)
+    ringed = tp == 2
+    if ringed:
+        proj, table = front(
+            layer_source_rows, entry_rescale_factor, sliding_mixer_entry_matrix,
+            recurrent_mixer_entry_matrix, latent_write_read_matrix,
+            timestep_matrix.reshape(width, 2 * heads), lane_forgetting_rate,
+            spike_forgetting_rate,
+        )
+        col_table = table.reshape(length, pairs, 8).transpose(1, 0, 2)
+        row_table = table.T.reshape(pairs, 8, length)
+        ends = table.reshape(length, heads, 4)
+        span_log = jnp.stack([ends[length - 1, :, 2], ends[0, :, 3]], axis=1)
+    else:
+        block = jnp.concatenate(
+            [sliding_mixer_entry_matrix[i] for i in range(3)]
+            + [recurrent_mixer_entry_matrix[i] for i in range(2)]
+            + [latent_write_read_matrix[i] for i in range(2)],
+            axis=1,
+        )
+        gathered = gather_rows(block)
+        weights = gathered.reshape(n * block.shape[0], block.shape[1])
+
+        x32 = layer_source_rows.astype(F32)
+        normed = (
+            x32
+            * lax.rsqrt(jnp.mean(x32 * x32, axis=-1, keepdims=True) + epsilon)
+            * entry_rescale_factor.astype(F32)
+        ).astype(BF16)
+        up = [(i, i + 1) for i in range(n - 1)]
+        down = [(i + 1, i) for i in range(n - 1)]
+        before = lax.ppermute(normed[own_rows - HALO :], "sp", up)
+        after = lax.ppermute(normed[:HALO], "sp", down)
+        shared = lax.all_gather(jnp.concatenate([before, normed, after], axis=0), "tp", axis=0)
+        rows = jnp.concatenate(
+            [shared[tp - 1, :HALO]]
+            + [shared[i, HALO : HALO + own_rows] for i in range(tp)]
+            + [shared[0, HALO + own_rows :]],
+            axis=0,
+        )
+
+        step_weight = timestep_matrix.reshape(width, 2 * heads)
+        raw = jnp.dot(rows, step_weight, preferred_element_type=F32).astype(BF16)
+        raw = raw[HALO : HALO + length].astype(F32).reshape(length, 2, heads)
+        deltas = jax.nn.softplus(raw)
+        logs = -deltas * lane_forgetting_rate[None] + spike_forgetting_rate[:, None, :]
+        tri = (jnp.arange(length)[:, None] >= jnp.arange(length)[None, :]).astype(F32)
+        run_f = jnp.dot(tri, logs[:, 0], precision=HIGHEST)
+        run_b = jnp.dot(tri.T, logs[:, 1], precision=HIGHEST)
+        table = jnp.stack([deltas[:, 0], deltas[:, 1], run_f, run_b], axis=2)
+        col_table = table.reshape(length, pairs, 8).transpose(1, 0, 2)
+        row_table = table.reshape(length, pairs, 8).transpose(1, 2, 0)
+        span_log = jnp.stack([run_f[length - 1], run_b[0]], axis=1)
+        exit_c, exit_s, weights = lax.optimization_barrier(
+            (sliding_mixer_exit_matrix, recurrent_mixer_exit_matrix, weights)
+        )
+        proj = project(rows, weights)
+        exit_c = lax.all_gather(exit_c, "sp", axis=1, tiled=True)
+        exit_s = lax.all_gather(exit_s, "sp", axis=1, tiled=True)
 
     latent = latent_kernel_coefficients
     pw, sw = 2 * HEAD_DIM, 2 * STATE
@@ -422,7 +895,13 @@
         col_table, row_table,
     )
 
-    entering = exchange_states(states.reshape(n, share, STATE), span_log)
+    states = states.reshape(n, share, STATE)
+    if ringed:
+        entering, exit_c, exit_s = exchange_exit(
+            states, span_log, sliding_mixer_exit_matrix, recurrent_mixer_exit_matrix
+        )
+    else:
+        entering = exchange_states(states, span_log)
     entering = entering.reshape(pairs * sw, STATE)
 
     y_ssd = pl.pallas_call(

time: 240 us -> 212 us (0.88)
  waiting for transfers between devices: 39.3 us -> 16.1 us
  Pallas kernels: 148 us -> 171 us
  between operations: 13.4 us -> 0.07 us
  starting transfers between devices: 7.44 us -> 1.53 us
  other arithmetic: 4.66 us -> 0.01 us
    pallas_call x3 -> x2, Pallas kernels: 133 us -> 156 us  [the longest x1 110 us: front(): pl.pallas_call(functools.partial(front_kernel, n), out_shape=[jax.ShapeDt...]
    all_gather x3 -> x0, waiting for transfers between devices: 20.3 us -> none  [the longest x1 20.3 us: local(): exit_s = lax.all_gather(exit_s, 'sp', axis=1, tiled=True)]
    ppermute x2 -> x0, starting transfers between devices: 5.83 us -> none  [the longest x1 3.77 us: local(): after = lax.ppermute(normed[:HALO], 'sp', down)]
    unnamed x37 -> x10, local copies, waits for them, and re-layouts: 7.44 us -> 2.14 us
    reshape x0 -> x3, local copies, waits for them, and re-layouts: none -> 3.16 us  [the longest x1 1.84 us: local(): timestep_matrix.reshape(width, 2 * heads)]
  transfers between devices with their start and end apart: 6 -> 1, of which waited for: 3 -> 1; matrix products, arithmetic and copies ran while one was open for 5% -> 1% of each run, Pallas kernels for 62% -> 0%
where the time goes in v1:
time: 212 us; the launch traced here: 210 us
  Pallas kernels  171 us (81%)
  waiting for transfers between devices  16.1 us (8%)
  local copies, waits for them, and re-layouts  10.7 us (5%)
  matrix products  10.6 us (5%)
    pallas_call x1, Pallas kernels, front(): pl.pallas_call(functools.partial(front_kernel, n), out_shape=[jax.ShapeDt...  110 us
    pallas_call x1, Pallas kernels, exchange_exit(): pl.pallas_call(functools.partial(exchange_exit_kernel, n, share), out_sha...  46.1 us
    ppermute x1, waiting for transfers between devices, local(): arrived = lax.ppermute(away, 'tp', [(0, 1), (1, 0)])  16.1 us
    pallas_call x1, Pallas kernels, local(): pl.pallas_call(mix_kernel, grid=(pairs,), in_specs=[pl.BlockSpec((full, c...  10.2 us
    dot_general x2, matrix products, partial(): jnp.dot(y_c, exit_c, preferred_element_type=F32)  5.84 us
    pallas_call x1, Pallas kernels, local(): pl.pallas_call(finish_kernel, grid=(pairs,), in_specs=[pl.BlockSpec((leng...  5.34 us
    dot_general x2, matrix products, partial(): jnp.dot(y_s, exit_s, preferred_element_type=F32)  4.75 us
  transfers between devices with their start and end apart: 1, of which 1 were waited for; matrix products, arithmetic and copies ran while one was open for 1% of the time, Pallas kernels for 0%

profile of v1, /device:TPU:12, one launch (start us, length us, event | category | flops | bytes accessed | tf_op | source)
XLA Modules:
  0.0 210.4 jit_solution(2141668044791426505)
XLA Ops:
  0.0 1.8 copy.28.step_ref
  1.8 1.5 copy.29.spike_ref
  3.4 1.3 reshape.29.gain_ref
  4.6 0.0 copy-start.2
  4.6 0.0 copy-start.3
  4.6 109.6 %shard_map.136 = (bf16[416,4608]{1,0:T(8,128)(2,1)}, f32[384,32]{1,0:T(8,128)}) custom-call(bf16[192,2048]{1,0:T(8,128)(2,1)} %x_ref.2, bf16[1,2048]{1,0:T(2,128)(2,1)} %reshape.29.gain_ref, bf16[3,128,512]{2,1,0:T(8,128)(2,1)} %conv_ref.1, bf16[2,128,512]{2,1,0:T(8,128)(2,1)} %rec_ref.1, bf16[2,128,1024]{2,1,0:T(8,128)(2,1)} %lat_ref.1, ...), custom_call_target="tpu_custom_call" | custom-call | flops 7851737088 | bytes 18874368 | tf_op jit(solution)/shard_map/pallas_call | solution.py:532
  114.3 1.0 copy.30
  115.3 1.2 copy.31
  116.5 1.7 copy.32
  118.1 0.0 copy-done.2
  118.2 0.6 copy.35
  118.8 0.2 slice_reduce_fusion.1
  119.0 0.1 copy.34
  119.1 0.1 broadcast_in_dim.7
  119.2 0.0 copy-done.3
  119.2 0.5 reshape.37.gain_ref
  119.7 10.2 %shard_map.137 = (bf16[384,512]{1,0:T(8,128)(2,1)}, f32[384,512]{1,0:T(8,128)}, bf16[384,1024]{1,0:T(8,128)(2,1)}, bf16[1024,128]{1,0:T(8,128)(2,1)}) custom-call(bf16[416,4608]{1,0:T(8,128)(2,1)} %get-tuple-element.14.og_ref.ig_ref.va_ref.x_ref.b_ref.c_ref.gate_ref, bf16[416,4608]{1,0:T(8,128)(2,1)} %get-tuple-element.14.og_ref.ig_ref.va_ref.x_ref.b_ref.c_ref.gate_ref, ...), custom_call_target="tpu_custom_call" | custom-call | flops 1207959552 | bytes 16777216 | tf_op jit(solution)/shard_map/pallas_call | solution.py:859
  129.9 0.7 broadcast_in_dim.8.l_ref
  130.6 46.1 %shard_map.138 = (bf16[16,64,128]{2,1,0:T(8,128)(2,1)}, bf16[512,2048]{1,0:T(8,128)(2,1)}, bf16[512,2048]{1,0:T(8,128)(2,1)}) custom-call(bf16[16,64,128]{2,1,0:T(8,128)(2,1)} %bitcast.24, f32[16,8,128]{2,1,0:T(8,128)} %broadcast_in_dim.8.l_ref, bf16[512,128]{1,0:T(8,128)(2,1)} %c_ref.1, bf16[512,128]{1,0:T(8,128)(2,1)} %x_ref.3), custom_call_target="tpu_custom_call" | custom-call | bytes 33554432 | tf_op jit(solution)/shard_map/pallas_call | solution.py:706
  176.8 3.6 %fusion.4 = f32[192,2048]{1,0:T(8,128)} fusion(bf16[512,2048]{1,0:T(8,128)(2,1)} %get-tuple-element.18, bf16[384,512]{1,0:T(8,128)(2,1)} %get-tuple-element.16, s32[]{:T(128)S(6)} %select_n.9), kind=kOutput, calls=%fused_computation.7 | convolution fusion | flops 402653184 | bytes 3866628 | tf_op jit(solution)/shard_map/dot_general | solution.py:924
  180.3 0.0 copy-start
  180.3 5.3 %shard_map.139 = bf16[384,512]{1,0:T(8,128)(2,1)} custom-call(f32[384,512]{1,0:T(8,128)} %get-tuple-element.19.within_ref, bf16[384,1024]{1,0:T(8,128)(2,1)} %get-tuple-element.20.reads_ref, bf16[1024,128]{1,0:T(8,128)(2,1)} %bitcast.23, bf16[416,4608]{1,0:T(8,128)(2,1)} %get-tuple-element.14.og_ref.ig_ref.va_ref.x_ref.b_ref.c_ref.gate_ref, ...), custom_call_target="tpu_custom_call" | custom-call | tf_op jit(solution)/shard_map/pallas_call | solution.py:907
  185.7 0.0 copy-done
  185.7 2.1 %fusion.2 = bf16[192,2048]{1,0:T(8,128)(2,1)S(1)} fusion(f32[192,2048]{1,0:T(8,128)} %fusion.4, bf16[512,2048]{1,0:T(8,128)(2,1)S(1)} %copy-done, bf16[384,512]{1,0:T(8,128)(2,1)} %shard_map.139, s32[]{:T(128)S(6)} %select_n.9), kind=kOutput, calls=%fused_computation.4 | convolution fusion | flops 403439616 | bytes 4653060 | tf_op jit(solution)/shard_map/dot_general | solution.py:925
  187.8 0.0 copy-start.1
  187.8 1.5 collective-permute-start
  189.3 2.3 %fusion.9 = f32[192,2048]{1,0:T(8,128)S(1)} fusion(bf16[512,2048]{1,0:T(8,128)(2,1)} %get-tuple-element.18, bf16[384,512]{1,0:T(8,128)(2,1)} %get-tuple-element.16, s32[]{:T(128)S(6)} %select_n.8), kind=kOutput, calls=%fused_computation.10 | convolution fusion | flops 402653184 | bytes 3866628 | tf_op jit(solution)/shard_map/dot_general | solution.py:924
  191.6 16.1 %collective-permute-done = bf16[192,2048]{1,0:T(8,128)(2,1)} collective-permute-done((bf16[192,2048]{1,0:T(8,128)(2,1)S(1)}, bf16[192,2048]{1,0:T(8,128)(2,1)}, u32[]{:S(2)}, u32[]{:S(2)}) %collective-permute-start) | collective-permute-done | bytes 786464 | tf_op jit(solution)/shard_map/ppermute | solution.py:938
  207.8 0.0 copy-done.1
  207.8 2.6 %add_convert_fusion = bf16[192,2048]{1,0:T(8,128)(2,1)} fusion(bf16[192,2048]{1,0:T(8,128)(2,1)} %collective-permute-done, f32[192,2048]{1,0:T(8,128)S(1)} %fusion.9, bf16[512,2048]{1,0:T(8,128)(2,1)S(1)} %copy-done, bf16[384,512]{1,0:T(8,128)(2,1)S(1)} %copy-done.1, s32[]{:T(128)S(6)} %select_n.8), kind=kOutput, calls=%fused_computation.5 | convolution fusion | flops 405012480 | bytes 5439492 | tf_op jit(solution)/shard_map/dot_general | solution.py:925
  (2 shorter events, 0.0 us)
Async XLA Ops:
  4.6 113.5 %copy-start.2 = (bf16[5,2,1024]{2,1,0:T(2,128)(2,1)S(1)}, bf16[5,2,1024]{2,1,0:T(2,128)(2,1)}, u32[]{:S(2)}) copy-start(bf16[5,2,1024]{2,1,0:T(2,128)(2,1)} %param.22) | copy-start | bytes 61444
  4.6 114.5 %copy-start.3 = (bf16[512]{0:T(512)(128)(2,1)S(1)}, bf16[512]{0:T(512)(128)(2,1)}, u32[]{:S(2)}) copy-start(bf16[512]{0:T(512)(128)(2,1)} %param.25) | copy-start | bytes 3076
  180.3 5.3 %copy-start = (bf16[512,2048]{1,0:T(8,128)(2,1)S(1)}, bf16[512,2048]{1,0:T(8,128)(2,1)}, u32[]{:S(2)}) copy-start(bf16[512,2048]{1,0:T(8,128)(2,1)} %get-tuple-element.22) | copy-start | bytes 6291460
  187.8 20.0 %copy-start.1 = (bf16[384,512]{1,0:T(8,128)(2,1)S(1)}, bf16[384,512]{1,0:T(8,128)(2,1)}, u32[]{:S(2)}) copy-start(bf16[384,512]{1,0:T(8,128)(2,1)} %shard_map.139) | copy-start | bytes 1179652
  187.8 20.0 %collective-permute-start = (bf16[192,2048]{1,0:T(8,128)(2,1)S(1)}, bf16[192,2048]{1,0:T(8,128)(2,1)}, u32[]{:S(2)}, u32[]{:S(2)}) collective-permute-start(bf16[192,2048]{1,0:T(8,128)(2,1)S(1)} %fusion.2), channel_id=1, source_target_pairs={{0,1},{1,0},{2,3},{3,2},{4,5},{5,4},{6,7},{7,6},{8,9},{9,8},{10,11... | collective-permute-start | bytes 2359304 | tf_op jit(solution)/shard_map/ppermute | solution.py:938

commit v2 on v1

--- a/solution.py
+++ b/solution.py
@@ -11,6 +11,8 @@
 STATE = 128
 HALO = 16
 CHUNKS = 2
+EARLY = 2
+BLOCKS = 4
 epsilon = 1e-05
 F32 = jnp.float32
 BF16 = jnp.bfloat16
@@ -299,7 +301,7 @@
 
 def front_kernel(
     n, x_ref, gain_ref, conv_ref, rec_ref, lat_ref, step_ref, rate_ref, spike_ref,
-    proj_ref, table_ref,
+    proj_ref, table_ref, turned_ref, ends_ref,
     w_buf, raw, normed, acc, own_sems, x_own, x_send, x_recv,
     ring_send, ring_recv, mate_send, mate_recv,
 ):
@@ -407,39 +409,6 @@
     def _():
         raw[HALO + length :, :] = jnp.zeros((HALO, width), BF16)
 
-    here.wait()
-    across.wait()
-
-    @pl.when(me > 0)
-    def _():
-        halo(0, True).wait_recv()
-
-    @pl.when(me < n - 1)
-    def _():
-        halo(0, False).wait_recv()
-
-    @pl.when(sends_up)
-    def _():
-        for t in range(2):
-            halo(t, True).wait_send()
-
-    @pl.when(sends_down)
-    def _():
-        for t in range(2):
-            halo(t, False).wait_send()
-
-    gain = gain_ref[...].astype(F32)
-    tall = 2 * HALO
-
-    def norm_block(i, _):
-        at = pl.ds(pl.multiple_of(i * tall, tall), tall)
-        x32 = raw[at, :].astype(F32)
-        scale = lax.rsqrt(jnp.mean(x32 * x32, axis=-1, keepdims=True) + epsilon)
-        normed[at, :] = (x32 * scale * gain).astype(BF16)
-        return 0
-
-    lax.fori_loop(0, raw.shape[0] // tall, norm_block, 0)
-
     def dot_part(step, way, chunk, first=False):
         start = pl.multiple_of((owner_of(step, way) - core) * depth, 2 * depth)
         span = pl.ds(start, 2 * depth)
@@ -459,28 +428,68 @@
 
         mate_copy(step + 1, way, chunk).start()
 
+    for step in range(EARLY):
+        for way, chunk in parts:
+            forward(step, way, chunk)
+    here.wait()
+    across.wait()
+
+    @pl.when(me > 0)
+    def _():
+        halo(0, True).wait_recv()
+
+    @pl.when(me < n - 1)
+    def _():
+        halo(0, False).wait_recv()
+
+    @pl.when(sends_up)
+    def _():
+        for t in range(2):
+            halo(t, True).wait_send()
+
+    @pl.when(sends_down)
+    def _():
+        for t in range(2):
+            halo(t, False).wait_send()
+
+    gain = gain_ref[...].astype(F32)
+    tall = 2 * HALO
+
+    def norm_block(i, _):
+        at = pl.ds(pl.multiple_of(i * tall, tall), tall)
+        x32 = raw[at, :].astype(F32)
+        scale = lax.rsqrt(jnp.mean(x32 * x32, axis=-1, keepdims=True) + epsilon)
+        normed[at, :] = (x32 * scale * gain).astype(BF16)
+        return 0
+
+    lax.fori_loop(0, raw.shape[0] // tall, norm_block, 0)
+
     for way, chunk in parts:
-        forward(0, way, chunk)
-    for way, chunk in parts:
+        forward(EARLY, way, chunk)
         mate_copy(0, way, chunk, True).wait_recv()
         dot_part(0, way, chunk, True)
 
-    heads = spike_ref.shape[1]
-    raw_step = jnp.dot(
-        normed[HALO : HALO + length, :], step_ref[...], preferred_element_type=F32
+    heads = spike_ref.shape[0]
+    raw_step = lax.dot_general(
+        normed[HALO : HALO + length, :], step_ref[...],
+        (((1,), (1,)), ((), ())), preferred_element_type=F32,
     ).astype(BF16)
-    row = lax.broadcasted_iota(jnp.int32, (2 * heads, 4 * heads), 0)
-    col = lax.broadcasted_iota(jnp.int32, (2 * heads, 4 * heads), 1)
+    lanes = table_ref.shape[1]
+    row = lax.broadcasted_iota(jnp.int32, (2 * heads, lanes), 0)
+    col = lax.broadcasted_iota(jnp.int32, (2 * heads, lanes), 1)
     pick = jnp.where((row % heads == col // 4) & (row // heads == col % 2), 1.0, 0.0)
-    head_row = lax.broadcasted_iota(jnp.int32, (heads, 4 * heads), 0)
-    head_col = lax.broadcasted_iota(jnp.int32, (heads, 4 * heads), 1)
+    head_row = lax.broadcasted_iota(jnp.int32, (heads, lanes), 0)
+    head_col = lax.broadcasted_iota(jnp.int32, (heads, lanes), 1)
     spread = jnp.where(head_row == head_col // 4, 1.0, 0.0).astype(F32)
     deltas = softplus(jnp.dot(raw_step, pick.astype(BF16), preferred_element_type=F32))
     rates = jnp.dot(rate_ref[...], spread, precision=HIGHEST, preferred_element_type=F32)
-    side = lax.broadcasted_iota(jnp.int32, (2, 4 * heads), 0)
-    kind2 = lax.broadcasted_iota(jnp.int32, (2, 4 * heads), 1) % 2
+    side = lax.broadcasted_iota(jnp.int32, (2, lanes), 0)
+    kind2 = lax.broadcasted_iota(jnp.int32, (2, lanes), 1) % 2
     rates = jnp.sum(jnp.where(side == kind2, rates, 0.0), axis=0, keepdims=True)
-    spikes = jnp.dot(spike_ref[...], spread, precision=HIGHEST, preferred_element_type=F32)
+    spikes = lax.dot_general(
+        spike_ref[...], spread, (((0,), (0,)), ((), ())),
+        precision=HIGHEST, preferred_element_type=F32,
+    )
     logs = spikes - deltas * rates
     t_at = lax.broadcasted_iota(jnp.int32, (length, length), 0)
     s_at = lax.broadcasted_iota(jnp.int32, (length, length), 1)
@@ -488,17 +497,37 @@
     run_f = jnp.dot(tri, logs, precision=HIGHEST, preferred_element_type=F32)
     tri = jnp.where(t_at <= s_at, 1.0, 0.0).astype(F32)
     run_b = jnp.dot(tri, logs, precision=HIGHEST, preferred_element_type=F32)
-    kind = lax.broadcasted_iota(jnp.int32, (length, 4 * heads), 1) % 4
-    table_ref[...] = jnp.where(kind < 2, deltas, jnp.where(kind == 2, run_f, run_b))
+    kind = lax.broadcasted_iota(jnp.int32, (length, lanes), 1) % 4
+    table = jnp.where(kind < 2, deltas, jnp.where(kind == 2, run_f, run_b))
+    table_ref[...] = table
+    turned_ref[...] = table.T
+    ends = jnp.where(kind[0:1] == 2, run_f[length - 1 : length], run_b[0:1])
+    ends_ref[...] = jnp.broadcast_to(ends, ends_ref.shape)
 
     def ring_step(step, _):
+        for way, chunk in parts:
+            forward(step, way, chunk)
+            mate_copy(step - EARLY, way, chunk, True).wait_recv()
+            dot_part(step - EARLY, way, chunk)
+        return 0
+
+    def catch_up(step, _):
+        for way, chunk in parts:
+            mate_copy(step, way, chunk, True).wait_recv()
+            dot_part(step, way, chunk)
+        return 0
+
+    lax.fori_loop(EARLY + 1, 2 * EARLY + 1, ring_step, 0)
+    lax.fori_loop(EARLY + 1, 2 * EARLY + 1, catch_up, 0)
+
+    def late_step(step, _):
         for way, chunk in parts:
             forward(step, way, chunk)
             mate_copy(step, way, chunk, True).wait_recv()
             dot_part(step, way, chunk)
         return 0
 
-    lax.fori_loop(1, chips - 1, ring_step, 0)
+    lax.fori_loop(2 * EARLY + 1, chips - 1, late_step, 0)
     for way, chunk in parts:
         mate_copy(chips - 1, way, chunk, True).wait_recv()
         dot_part(chips - 1, way, chunk)
@@ -526,17 +555,20 @@
     depth = conv_w.shape[1]
     cols = sum(w.shape[0] * w.shape[2] for w in (conv_w, rec_w, lat_w))
     blocks = sum(w.shape[0] for w in (conv_w, rec_w, lat_w))
-    heads = spike.shape[1]
+    heads = spike.shape[0]
+    assert 4 * heads <= STATE and 2 * EARLY + 1 < chips
     vmem = pl.BlockSpec(memory_space=pltpu.VMEM)
     hbm = pl.BlockSpec(memory_space=pl.ANY)
     return pl.pallas_call(
         functools.partial(front_kernel, n),
         out_shape=[
             jax.ShapeDtypeStruct((full, cols), BF16),
-            jax.ShapeDtypeStruct((length, 4 * heads), F32),
+            jax.ShapeDtypeStruct((length, STATE), F32),
+            jax.ShapeDtypeStruct((STATE, length), F32),
+            jax.ShapeDtypeStruct((8, STATE), F32),
         ],
         in_specs=[vmem, vmem, hbm, hbm, hbm, vmem, vmem, vmem],
-        out_specs=[vmem, vmem],
+        out_specs=[vmem] * 4,
         scratch_shapes=[
             pltpu.VMEM((n * depth, cols), BF16),
             pltpu.VMEM((full, width), BF16),
@@ -636,94 +668,265 @@
     return chips, start, advance, finish
 
 
-def exchange_exit_kernel(
-    n, share, s_ref, l_ref, c_ref, x_ref, out_ref, c_out, x_out,
-    got, logs, enter, s_sem, s_in, l_out, l_in, e_out, e_in,
+def tap_sum(padded, taps, length):
+    full = padded.shape[0]
+    half = len(taps) // 2
+    total = None
+    for k, tap in enumerate(taps):
+        moved = padded if k == half else pltpu.roll(padded, (half - k) % full, 0)
+        term = moved[HALO : HALO + length] * tap
+        total = term if total is None else total + term
+    return total
+
+
+def tail_kernel(
+    n, proj_ref, table_ref, turned_ref, ends_ref, ct_ref, xt_ref, lt_ref, gain_ref,
+    c_ref, x_ref, out_ref,
+    c_all, x_all, y_c, y_s, within, reads, states, got, logs, enter, entered, away, came,
+    s_out, s_in, l_out, l_in, e_out, e_in, p_out, p_in,
     own_sems, ring_send, ring_recv, mate_send, mate_recv,
 ):
     me = lax.axis_index("sp")
+    tp_me = lax.axis_index("tp")
+    length = y_c.shape[0]
+    own_rows, width = out_ref.shape
+    conv_width, ssd_width = y_c.shape[1], y_s.shape[1]
+    state_width = reads.shape[1]
+    pairs = ssd_width // (2 * HEAD_DIM)
+    cw, pw, sw = conv_width // pairs, 2 * HEAD_DIM, 2 * STATE
+    at_gate = 3 * conv_width
+    at_x = at_gate + ssd_width
+    at_b = at_x + ssd_width
+    at_c = at_b + state_width
+
     barrier = pltpu.get_barrier_semaphore()
+    for other in [{"sp": (me + k) % n} for k in range(1, n)] + [{"tp": 1 - tp_me}]:
+        pl.semaphore_signal(
+            barrier, inc=1, device_id=other, device_id_type=pl.DeviceIdType.MESH
+        )
+    pl.semaphore_wait(barrier, n)
+    chips, start, advance, finish = exit_ring(
+        n, c_ref, x_ref, c_all, x_all, own_sems, (ring_send, ring_recv, mate_send, mate_recv)
+    )
+    start()
+
+    def log_copy(k, incoming=False):
+        there = (me + n - k) % n if incoming else (me + k) % n
+        slot = there if incoming else me
+        return send_to(ends_ref, logs.at[slot], l_out.at[k], l_in.at[k], {"sp": there})
+
     for k in range(1, n):
-        pl.semaphore_signal(
-            barrier,
-            inc=1,
-            device_id={"sp": (me + k) % n},
-            device_id_type=pl.DeviceIdType.MESH,
-        )
-    pl.semaphore_wait(barrier, n - 1)
-    chips, start, advance, finish = exit_ring(
-        n, c_ref, x_ref, c_out, x_out, own_sems, (ring_send, ring_recv, mate_send, mate_recv)
-    )
-
-    def copy(src, dst, out_sem, in_sem, k, there, slot):
+        log_copy(k).start()
+    logs[me] = ends_ref[...]
+
+    t_at = lax.broadcasted_iota(jnp.int32, (length, length), 0)
+    s_at = lax.broadcasted_iota(jnp.int32, (length, length), 1)
+    below, above = t_at > s_at, t_at < s_at
+    here = slice(HALO, HALO + length)
+
+    def rows_f32(ref, j, wide, base):
+        return ref[:, base + j * wide : base + (j + 1) * wide].astype(F32)
+
+    def state_copy(owner):
         return send_to(
-            src.at[there], dst.at[slot], out_sem.at[k], in_sem.at[k], {"sp": there}
-        )
+            states.at[owner], got.at[me], s_out.at[owner], s_in.at[me], {"sp": owner}
+        )
+
+    def mix_pair(j):
+        taps = ct_ref[:, j * cw : (j + 1) * cw].astype(F32)
+        gated = rows_f32(proj_ref, j, cw, conv_width) * rows_f32(proj_ref, j, cw, 2 * conv_width)
+        conv = tap_sum(
+            gated.astype(BF16).astype(F32), [taps[k : k + 1] for k in range(taps.shape[0])], length
+        )
+        og = proj_ref[here, j * cw : (j + 1) * cw].astype(F32)
+        y_c[:, j * cw : (j + 1) * cw] = (og * conv).astype(BF16)
+        taps = xt_ref[:, j * pw : (j + 1) * pw].astype(F32)
+        xs = silu(
+            tap_sum(
+                rows_f32(proj_ref, j, pw, at_x), [taps[k : k + 1] for k in range(taps.shape[0])], length
+            )
+        ).astype(BF16)
+        taps = [lt_ref[k, :, j * sw : (j + 1) * sw].astype(F32) for k in range(lt_ref.shape[0])]
+        bs = silu(
+            tap_sum(rows_f32(proj_ref, j, sw, at_b), [tap[0:1] for tap in taps], length)
+        ).astype(BF16)
+        cs = silu(
+            tap_sum(rows_f32(proj_ref, j, sw, at_c), [tap[1:2] for tap in taps], length)
+        ).astype(BF16)
+        reads[:, j * sw : (j + 1) * sw] = cs
+        outs = []
+        for h in range(2):
+            c_h = cs[:, h * STATE : (h + 1) * STATE]
+            b_h = bs[:, h * STATE : (h + 1) * STATE]
+            x_h = xs[:, h * HEAD_DIM : (h + 1) * HEAD_DIM]
+            head = 2 * j + h
+            cols = table_ref[:, 4 * head : 4 * head + 4]
+            rows = turned_ref[4 * head : 4 * head + 4, :]
+            scores = lax.dot_general(
+                c_h, b_h, (((1,), (1,)), ((), ())), preferred_element_type=F32
+            )
+            gap = jnp.where(above, cols[:, 3:4] - rows[3:4], cols[:, 2:3] - rows[2:3])
+            d_f, d_b = rows[0:1], rows[1:2]
+            scale = jnp.where(below, d_f, jnp.where(above, d_b, d_f + d_b))
+            w = (scores * jnp.exp(gap) * scale).astype(BF16)
+            outs.append(jnp.dot(w, x_h, preferred_element_type=F32))
+            x32 = x_h.astype(F32)
+            end_f = jnp.exp(rows[2:3, length - 1 : length] - cols[:, 2:3])
+            end_b = jnp.exp(rows[3:4, 0:1] - cols[:, 3:4])
+            both = jnp.concatenate(
+                [x32 * (end_f * cols[:, 0:1]), x32 * (end_b * cols[:, 1:2])], axis=1
+            ).astype(BF16)
+            state = lax.dot_general(
+                both, b_h, (((0,), (0,)), ((), ())), preferred_element_type=F32
+            ).astype(BF16)
+            for d in range(2):
+                states[2 * head + d] = state[d * HEAD_DIM : (d + 1) * HEAD_DIM]
+        within[:, j * pw : (j + 1) * pw] = jnp.concatenate(outs, axis=1)
+
+    def send_states(j):
+        for owner in range(4 * j, 4 * j + 4):
+            @pl.when(me != owner)
+            def _():
+                state_copy(owner).start()
+
+            @pl.when(me == owner)
+            def _():
+                got[owner] = states[owner]
+
+    for j in range(pairs):
+        mix_pair(j)
+        advance(j)
+        send_states(j)
 
     for k in range(1, n):
-        there = (me + k) % n
-        copy(s_ref, got, s_sem, s_in, k, there, me).start()
-        copy(l_ref, logs, l_out, l_in, k, there, me).start()
-    start()
-    got[me] = s_ref[me]
-    logs[me] = l_ref[me]
-    advance(0)
-    advance(1)
+        log_copy(k, True).wait_recv()
+    lane = 4 * (me // 2) + 2 + me % 2
+    lane_at = lax.broadcasted_iota(jnp.int32, (1, STATE), 1)
     for k in range(1, n):
-        here = (me + n - k) % n
-        copy(s_ref, got, s_sem, s_in, k, here, here).wait_recv()
-        copy(l_ref, logs, l_out, l_in, k, here, here).wait_recv()
-    back = (me * share // HEAD_DIM) % 2
-    acc = jnp.zeros(s_ref.shape[1:], F32)
+        other = (me + k) % n
+        send_to(
+            states.at[other], got.at[other], s_out.at[other], s_in.at[other], {"sp": other}
+        ).wait_recv()
+    back = me % 2
+    acc = jnp.zeros(got.shape[1:], F32)
     for i in range(n):
         j = back * (n - 1 - i) + (1 - back) * i
         enter[j] = acc.astype(BF16)
-        acc = acc * jnp.exp(logs[j][0:1, :]) + got[j].astype(F32)
-    out_ref[me] = enter[me]
+        log = jnp.sum(
+            jnp.where(lane_at == lane, logs[j][0:1, :], 0.0), axis=1, keepdims=True
+        )
+        acc = acc * jnp.exp(log) + got[j].astype(F32)
+    entered[me] = enter[me]
+
+    def enter_copy(k, incoming=False):
+        there = (me + n - k) % n if incoming else (me + k) % n
+        slot = there if incoming else me
+        return send_to(enter.at[there], entered.at[slot], e_out.at[k], e_in.at[k], {"sp": there})
+
     for k in range(1, n):
-        copy(enter, out_ref, e_out, e_in, k, (me + k) % n, me).start()
-    for step in range(2, chips - 1):
+        enter_copy(k).start()
+    for step in range(pairs, chips - 1):
         advance(step)
     for k in range(1, n):
-        here = (me + n - k) % n
-        copy(enter, out_ref, e_out, e_in, k, here, here).wait_recv()
+        enter_copy(k, True).wait_recv()
+
+    for j in range(pairs):
+        outs = []
+        gate = silu(rows_f32(proj_ref, j, pw, at_gate)[here])
+        for h in range(2):
+            head = 2 * j + h
+            cols = table_ref[:, 4 * head : 4 * head + 4]
+            wide = jnp.concatenate([entered[2 * head], entered[2 * head + 1]], axis=0)
+            both = lax.dot_general(
+                reads[:, head * STATE : (head + 1) * STATE], wide,
+                (((1,), (1,)), ((), ())), preferred_element_type=F32,
+            )
+            mine = slice(h * HEAD_DIM, (h + 1) * HEAD_DIM)
+            y = within[:, head * HEAD_DIM : (head + 1) * HEAD_DIM]
+            y = y + both[:, :HEAD_DIM] * jnp.exp(cols[:, 2:3])
+            y = y + both[:, HEAD_DIM:] * jnp.exp(cols[:, 3:4])
+            g = y * gate[:, mine]
+            g = g * lax.rsqrt(jnp.mean(g * g, axis=-1, keepdims=True) + epsilon)
+            gain = gain_ref[:, head * HEAD_DIM : (head + 1) * HEAD_DIM].astype(F32)
+            outs.append(g * gain)
+        y_s[:, j * pw : (j + 1) * pw] = jnp.concatenate(outs, axis=1).astype(BF16)
+    finish()
+
+    part = width // BLOCKS
+
+    def partial(owner, block):
+        rows = pl.ds(pl.multiple_of(owner * own_rows, HALO), own_rows)
+        cols = slice(block * part, (block + 1) * part)
+        return jnp.dot(
+            y_c[rows, :], c_all[:, cols], preferred_element_type=F32
+        ) + jnp.dot(y_s[rows, :], x_all[:, cols], preferred_element_type=F32)
+
+    def partial_copy(block):
+        return send_to(
+            away.at[block], came.at[block], p_out.at[block], p_in.at[block], {"tp": 1 - tp_me}
+        )
+
+    for block in range(BLOCKS):
+        away[block] = partial(1 - tp_me, block).astype(BF16)
+        partial_copy(block).start()
+    for block in range(BLOCKS):
+        kept = partial(tp_me, block)
+        partial_copy(block).wait_recv()
+        cols = slice(block * part, (block + 1) * part)
+        out_ref[:, cols] = (kept + came[block].astype(F32)).astype(BF16)
+    for block in range(BLOCKS):
+        partial_copy(block).wait_send()
     for k in range(1, n):
-        there = (me + k) % n
-        copy(s_ref, got, s_sem, s_in, k, there, me).wait_send()
-        copy(l_ref, logs, l_out, l_in, k, there, me).wait_send()
-        copy(enter, out_ref, e_out, e_in, k, there, me).wait_send()
-    finish()
-
-
-def exchange_exit(states, span_log, exit_c, exit_s):
-    n, share, _ = states.shape
+        log_copy(k).wait_send()
+        enter_copy(k).wait_send()
+        other = (me + k) % n
+        state_copy(other).wait_send()
+
+
+def tail(proj, table, turned, ends, conv_taps, x_taps, latent_taps, gain, exit_c, exit_s, own_rows):
+    n = lax.axis_size("sp")
     chips = n // 2
-    assert HEAD_DIM % share == 0
-    tables = jnp.repeat(span_log.reshape(-1), HEAD_DIM // share)
-    tables = jnp.broadcast_to(tables[:, None, None], (n, 8, STATE))
-    wide = (exit_c.shape[0], exit_c.shape[1] * n)
+    length = table.shape[0]
+    conv_width, ssd_width = exit_c.shape[0], exit_s.shape[0]
+    state_width = latent_taps.shape[2]
+    width = exit_c.shape[1] * n
+    pairs = ssd_width // (2 * HEAD_DIM)
+    assert 4 * pairs == n and pairs < chips - 1 and conv_width == ssd_width
     vmem = pl.BlockSpec(memory_space=pltpu.VMEM)
+    spans = (n, HEAD_DIM, STATE)
+    blocks = (BLOCKS, own_rows, width // BLOCKS)
     return pl.pallas_call(
-        functools.partial(exchange_exit_kernel, n, share),
-        out_shape=[
-            jax.ShapeDtypeStruct(states.shape, BF16),
-            jax.ShapeDtypeStruct(wide, BF16),
-            jax.ShapeDtypeStruct(wide, BF16),
-        ],
-        in_specs=[vmem] * 4,
-        out_specs=[vmem] * 3,
+        functools.partial(tail_kernel, n),
+        out_shape=jax.ShapeDtypeStruct((own_rows, width), BF16),
+        in_specs=[vmem] * 10,
+        out_specs=vmem,
         scratch_shapes=[
-            pltpu.VMEM(states.shape, BF16),
-            pltpu.VMEM(tables.shape, F32),
-            pltpu.VMEM(states.shape, BF16),
+            pltpu.VMEM((conv_width, width), BF16),
+            pltpu.VMEM((ssd_width, width), BF16),
+            pltpu.VMEM((length, conv_width), BF16),
+            pltpu.VMEM((length, ssd_width), BF16),
+            pltpu.VMEM((length, ssd_width), F32),
+            pltpu.VMEM((length, state_width), BF16),
+            pltpu.VMEM(spans, BF16),
+            pltpu.VMEM(spans, BF16),
+            pltpu.VMEM((n, 8, STATE), F32),
+            pltpu.VMEM(spans, BF16),
+            pltpu.VMEM(spans, BF16),
+            pltpu.VMEM(blocks, BF16),
+            pltpu.VMEM(blocks, BF16),
         ]
         + [pltpu.SemaphoreType.DMA((n,))] * 6
+        + [pltpu.SemaphoreType.DMA((BLOCKS,))] * 2
         + [pltpu.SemaphoreType.DMA((2,))]
         + [pltpu.SemaphoreType.DMA((chips - 1, 2, CHUNKS))] * 2
         + [pltpu.SemaphoreType.DMA((chips, 2, CHUNKS))] * 2,
-        compiler_params=pltpu.CompilerParams(collective_id=3, has_side_effects=True),
-        cost_estimate=pl.CostEstimate(flops=0, bytes_accessed=2**25, transcendentals=0),
-    )(states, tables, exit_c, exit_s)
+        compiler_params=pltpu.CompilerParams(
+            collective_id=3, has_side_effects=True, vmem_limit_bytes=48 * 2**20
+        ),
+        cost_estimate=pl.CostEstimate(
+            flops=4 * length * conv_width * width, bytes_accessed=2**24, transcendentals=0
+        ),
+    )(proj, table, turned, ends, conv_taps, x_taps, latent_taps, gain, exit_c, exit_s)
 
 
 def project_kernel(r_ref, w_ref, o_ref):
@@ -791,64 +994,65 @@
     cw = conv_width // pairs
 
     share = heads * 2 * HEAD_DIM // n
-    ringed = tp == 2
-    if ringed:
-        proj, table = front(
+    if tp == 2 and 2 * heads == n:
+        proj, table, turned, ends = front(
             layer_source_rows, entry_rescale_factor, sliding_mixer_entry_matrix,
             recurrent_mixer_entry_matrix, latent_write_read_matrix,
-            timestep_matrix.reshape(width, 2 * heads), lane_forgetting_rate,
-            spike_forgetting_rate,
-        )
-        col_table = table.reshape(length, pairs, 8).transpose(1, 0, 2)
-        row_table = table.T.reshape(pairs, 8, length)
-        ends = table.reshape(length, heads, 4)
-        span_log = jnp.stack([ends[length - 1, :, 2], ends[0, :, 3]], axis=1)
-    else:
-        block = jnp.concatenate(
-            [sliding_mixer_entry_matrix[i] for i in range(3)]
-            + [recurrent_mixer_entry_matrix[i] for i in range(2)]
-            + [latent_write_read_matrix[i] for i in range(2)],
-            axis=1,
-        )
-        gathered = gather_rows(block)
-        weights = gathered.reshape(n * block.shape[0], block.shape[1])
-
-        x32 = layer_source_rows.astype(F32)
-        normed = (
-            x32
-            * lax.rsqrt(jnp.mean(x32 * x32, axis=-1, keepdims=True) + epsilon)
-            * entry_rescale_factor.astype(F32)
-        ).astype(BF16)
-        up = [(i, i + 1) for i in range(n - 1)]
-        down = [(i + 1, i) for i in range(n - 1)]
-        before = lax.ppermute(normed[own_rows - HALO :], "sp", up)
-        after = lax.ppermute(normed[:HALO], "sp", down)
-        shared = lax.all_gather(jnp.concatenate([before, normed, after], axis=0), "tp", axis=0)
-        rows = jnp.concatenate(
-            [shared[tp - 1, :HALO]]
-            + [shared[i, HALO : HALO + own_rows] for i in range(tp)]
-            + [shared[0, HALO + own_rows :]],
-            axis=0,
-        )
-
-        step_weight = timestep_matrix.reshape(width, 2 * heads)
-        raw = jnp.dot(rows, step_weight, preferred_element_type=F32).astype(BF16)
-        raw = raw[HALO : HALO + length].astype(F32).reshape(length, 2, heads)
-        deltas = jax.nn.softplus(raw)
-        logs = -deltas * lane_forgetting_rate[None] + spike_forgetting_rate[:, None, :]
-        tri = (jnp.arange(length)[:, None] >= jnp.arange(length)[None, :]).astype(F32)
-        run_f = jnp.dot(tri, logs[:, 0], precision=HIGHEST)
-        run_b = jnp.dot(tri.T, logs[:, 1], precision=HIGHEST)
-        table = jnp.stack([deltas[:, 0], deltas[:, 1], run_f, run_b], axis=2)
-        col_table = table.reshape(length, pairs, 8).transpose(1, 0, 2)
-        row_table = table.reshape(length, pairs, 8).transpose(1, 2, 0)
-        span_log = jnp.stack([run_f[length - 1], run_b[0]], axis=1)
-        exit_c, exit_s, weights = lax.optimization_barrier(
-            (sliding_mixer_exit_matrix, recurrent_mixer_exit_matrix, weights)
-        )
-        proj = project(rows, weights)
-        exit_c = lax.all_gather(exit_c, "sp", axis=1, tiled=True)
-        exit_s = lax.all_gather(exit_s, "sp", axis=1, tiled=True)
+            timestep_matrix.transpose(1, 2, 0).reshape(2 * heads, width),
+            lane_forgetting_rate, spike_forgetting_rate.T,
+        )
+        return tail(
+            proj, table, turned, ends, sliding_kernel_coefficients,
+            recurrent_kernel_coefficients, latent_kernel_coefficients,
+            lane_rescale_factor.reshape(1, -1), sliding_mixer_exit_matrix,
+            recurrent_mixer_exit_matrix, own_rows,
+        )
+
+    block = jnp.concatenate(
+        [sliding_mixer_entry_matrix[i] for i in range(3)]
+        + [recurrent_mixer_entry_matrix[i] for i in range(2)]
+        + [latent_write_read_matrix[i] for i in range(2)],
+        axis=1,
+    )
+    gathered = gather_rows(block)
+    weights = gathered.reshape(n * block.shape[0], block.shape[1])
+
+    x32 = layer_source_rows.astype(F32)
+    normed = (
+        x32
+        * lax.rsqrt(jnp.mean(x32 * x32, axis=-1, keepdims=True) + epsilon)
+        * entry_rescale_factor.astype(F32)
+    ).astype(BF16)
+    up = [(i, i + 1) for i in range(n - 1)]
+    down = [(i + 1, i) for i in range(n - 1)]
+    before = lax.ppermute(normed[own_rows - HALO :], "sp", up)
+    after = lax.ppermute(normed[:HALO], "sp", down)
+    shared = lax.all_gather(jnp.concatenate([before, normed, after], axis=0), "tp", axis=0)
+    rows = jnp.concatenate(
+        [shared[tp - 1, :HALO]]
+        + [shared[i, HALO : HALO + own_rows] for i in range(tp)]
+        + [shared[0, HALO + own_rows :]],
+        axis=0,
+    )
+
+    step_weight = timestep_matrix.reshape(width, 2 * heads)
+    raw = jnp.dot(rows, step_weight, preferred_element_type=F32).astype(BF16)
+    raw = raw[HALO : HALO + length].astype(F32).reshape(length, 2, heads)
+    deltas = jax.nn.softplus(raw)
+    logs = -deltas * lane_forgetting_rate[None] + spike_forgetting_rate[:, None, :]
+    tri = (jnp.arange(length)[:, None] >= jnp.arange(length)[None, :]).astype(F32)
+    run_f = jnp.dot(tri, logs[:, 0], precision=HIGHEST)
+    run_b = jnp.dot(tri.T, logs[:, 1], precision=HIGHEST)
+    table = jnp.stack([deltas[:, 0], deltas[:, 1], run_f, run_b], axis=2)
+    col_table = table.reshape(length, pairs, 8).transpose(1, 0, 2)
+    row_table = table.reshape(length, pairs, 8).transpose(1, 2, 0)
+    span_log = jnp.stack([run_f[length - 1], run_b[0]], axis=1)
+    exit_c, exit_s, weights = lax.optimization_barrier(
+        (sliding_mixer_exit_matrix, recurrent_mixer_exit_matrix, weights)
+    )
+    proj = project(rows, weights)
+    exit_c = lax.all_gather(exit_c, "sp", axis=1, tiled=True)
+    exit_s = lax.all_gather(exit_s, "sp", axis=1, tiled=True)
 
     latent = latent_kernel_coefficients
     pw, sw = 2 * HEAD_DIM, 2 * STATE
@@ -895,13 +1099,7 @@
         col_table, row_table,
     )
 
-    states = states.reshape(n, share, STATE)
-    if ringed:
-        entering, exit_c, exit_s = exchange_exit(
-            states, span_log, sliding_mixer_exit_matrix, recurrent_mixer_exit_matrix
-        )
-    else:
-        entering = exchange_states(states, span_log)
+    entering = exchange_states(states.reshape(n, share, STATE), span_log)
     entering = entering.reshape(pairs * sw, STATE)
 
     y_ssd = pl.pallas_call(

time: 212 us -> 179 us (0.84)
  waiting for transfers between devices: 16.1 us -> 0 us
  matrix products: 10.6 us -> 0 us
  local copies, waits for them, and re-layouts: 10.7 us -> 7.48 us
    ppermute x1 -> x0, waiting for transfers between devices: 16.1 us -> none  [local(): arrived = lax.ppermute(away, 'tp', [(0, 1), (1, 0)])]
    dot_general x4 -> x0, matrix products: 10.6 us -> none  [the longest x2 5.84 us: partial(): jnp.dot(y_c, exit_c, preferred_element_type=F32)]
    pallas_call x1, Pallas kernels: 110 us -> 101 us  [front(): pl.pallas_call(functools.partial(front_kernel, n), out_shape=[jax.ShapeDt...]
    pallas_call x3 -> x1, Pallas kernels: 61.7 us -> 70.3 us  [tail(): pl.pallas_call(functools.partial(tail_kernel, n), out_shape=jax.ShapeDtyp...]
    unnamed x10 -> x19, local copies, waits for them, and re-layouts: 2.14 us -> 5.51 us
    reshape x3 -> x0, local copies, waits for them, and re-layouts: 3.02 us -> none  [the longest x1 1.84 us: local(): timestep_matrix.reshape(width, 2 * heads)]
  transfers between devices with their start and end apart: 1 -> 0, of which waited for: 1 -> 0; matrix products, arithmetic and copies ran while one was open for 1% -> 0% of each run, Pallas kernels for 0% -> 0%
where the time goes in v2:
time: 179 us; the launch traced here: 178 us
  Pallas kernels  171 us (96%)
  local copies, waits for them, and re-layouts  7.48 us (4%)
    pallas_call x1, Pallas kernels, front(): pl.pallas_call(functools.partial(front_kernel, n), out_shape=[jax.ShapeDt...  101 us
    pallas_call x1, Pallas kernels, tail(): pl.pallas_call(functools.partial(tail_kernel, n), out_shape=jax.ShapeDtyp...  70.3 us
    unnamed x19, local copies, waits for them, and re-layouts  5.51 us

profile of v2, /device:TPU:12, one launch (start us, length us, event | category | flops | bytes accessed | tf_op | source)
XLA Modules:
  0.0 178.4 jit_solution(1911099415081557936)
XLA Ops:
  0.0 0.7 reshape.11.gain_ref
  0.7 1.3 reshape.9.gain_ref
  2.0 0.0 copy-start
  2.0 0.0 copy-start.1
  2.0 0.0 copy-start.2
  2.0 0.0 copy-start.3
  2.0 0.0 copy-start.4
  2.0 100.6 %shard_map.136 = (bf16[416,4608]{1,0:T(8,128)(2,1)}, f32[384,128]{1,0:T(8,128)}, f32[128,384]{1,0:T(8,128)}, f32[8,128]{1,0:T(8,128)}) custom-call(bf16[192,2048]{1,0:T(8,128)(2,1)} %x_ref.2, bf16[1,2048]{1,0:T(2,128)(2,1)} %reshape.9.gain_ref, bf16[3,128,512]{2,1,0:T(8,128)(2,1)} %conv_ref.1, bf16[2,128,512]{2,1,0:T(8,128)(2,1)} %rec_ref.1, ...), custom_call_target="tpu_custom_call" | custom-call | flops 7851737088 | bytes 18874368 | tf_op jit(solution)/shard_map/pallas_call | solution.py:562
  102.6 0.0 copy-done
  102.6 0.0 copy-done.1
  102.6 0.0 copy-done.2
  102.6 0.0 copy-done.3
  102.6 0.0 copy-done.4
  102.6 0.0 copy-start.5
  102.6 2.1 %copy-done.5 = bf16[416,4608]{1,0:T(8,128)(2,1)S(1)} copy-done((bf16[416,4608]{1,0:T(8,128)(2,1)S(1)}, bf16[416,4608]{1,0:T(8,128)(2,1)}, u32[]{:S(2)}) %copy-start.5) | copy-done | bytes 3833880
  104.7 0.0 copy-start.6
  104.7 0.9 copy-done.6
  105.6 0.0 copy-start.7
  105.6 0.9 copy-done.7
  106.6 0.0 copy-start.8
  106.6 0.7 copy-done.8
  107.2 70.3 %shard_map.137 = bf16[192,2048]{1,0:T(8,128)(2,1)S(1)} custom-call(bf16[416,4608]{1,0:T(8,128)(2,1)S(1)} %copy-done.5, f32[384,128]{1,0:T(8,128)S(1)} %copy-done.6, f32[128,384]{1,0:T(8,128)S(1)} %copy-done.7, f32[8,128]{1,0:T(8,128)S(1)} %copy-done.8, bf16[3,512]{1,0:T(4,128)(2,1)S(1)} %copy-done.4, bf16[5,512]{1,0:T(8,128)(2,1)S(1)} %copy-done.3, ...), custom_call_target="tpu_custom_call" | custom-call | flops 1610612736 | bytes 16777216 | tf_op jit(solution)/shard_map/pallas_call | solution.py:898
  177.6 0.9 copy.16
Async XLA Ops:
  2.0 100.6 %copy-start = (bf16[512,128]{1,0:T(8,128)(2,1)S(1)}, bf16[512,128]{1,0:T(8,128)(2,1)}, u32[]{:S(2)}) copy-start(bf16[512,128]{1,0:T(8,128)(2,1)} %c_ref.1) | copy-start | bytes 393220
  2.0 100.6 %copy-start.1 = (bf16[512,128]{1,0:T(8,128)(2,1)S(1)}, bf16[512,128]{1,0:T(8,128)(2,1)}, u32[]{:S(2)}) copy-start(bf16[512,128]{1,0:T(8,128)(2,1)} %x_ref.3) | copy-start | bytes 393220
  2.0 100.6 %copy-start.2 = (bf16[5,2,1024]{2,1,0:T(2,128)(2,1)S(1)}, bf16[5,2,1024]{2,1,0:T(2,128)(2,1)}, u32[]{:S(2)}) copy-start(bf16[5,2,1024]{2,1,0:T(2,128)(2,1)} %lt_ref.1) | copy-start | bytes 61444
  2.0 100.6 %copy-start.3 = (bf16[5,512]{1,0:T(8,128)(2,1)S(1)}, bf16[5,512]{1,0:T(8,128)(2,1)}, u32[]{:S(2)}) copy-start(bf16[5,512]{1,0:T(8,128)(2,1)} %xt_ref.1) | copy-start | bytes 15364
  2.0 100.6 %copy-start.4 = (bf16[3,512]{1,0:T(4,128)(2,1)S(1)}, bf16[3,512]{1,0:T(4,128)(2,1)}, u32[]{:S(2)}) copy-start(bf16[3,512]{1,0:T(4,128)(2,1)} %ct_ref.1) | copy-start | bytes 9220
  102.6 2.1 %copy-start.5 = (bf16[416,4608]{1,0:T(8,128)(2,1)S(1)}, bf16[416,4608]{1,0:T(8,128)(2,1)}, u32[]{:S(2)}) copy-start(bf16[416,4608]{1,0:T(8,128)(2,1)} %get-tuple-element.9.proj_ref) | copy-start | bytes 11501572
  104.7 0.9 copy-start.6
  105.6 0.9 copy-start.7
  106.6 0.7 copy-start.8

commit v3 on v0

--- a/solution.py
+++ b/solution.py
@@ -9,8 +9,11 @@
 
 HEAD_DIM = 64
 STATE = 128
-HALO = 8
+HALO = 16
 CHUNKS = 2
+LAG = 2
+SKEW = 2
+BLOCKS = 4
 epsilon = 1e-05
 F32 = jnp.float32
 BF16 = jnp.bfloat16
@@ -265,6 +268,605 @@
     )(states, tables)
 
 
+def ring_spot(n):
+    chips = n // 2
+    me = lax.axis_index("sp")
+    core, chip = me % 2, me // 2
+    odd = chip % 2
+    spot = (1 - odd) * (chip // 2) + odd * (chips - 1 - chip // 2)
+
+    def device(position):
+        position = (position + 2 * chips) % chips
+        half = (chips + 1) // 2
+        late = position // half
+        late_chip = 2 * (chips - 1 - position) + 1
+        return 2 * ((1 - late) * 2 * position + late * late_chip) + core
+
+    return me, core, spot, device
+
+
+def send_to(src, dst, out_sem, in_sem, target):
+    return pltpu.make_async_remote_copy(
+        src_ref=src,
+        dst_ref=dst,
+        send_sem=out_sem,
+        recv_sem=in_sem,
+        device_id=target,
+        device_id_type=pl.DeviceIdType.MESH,
+    )
+
+
+def softplus(v):
+    return jnp.maximum(v, 0.0) + jnp.log1p(jnp.exp(-jnp.abs(v)))
+
+
+def tap_sum(padded, taps, length):
+    full = padded.shape[0]
+    half = len(taps) // 2
+    total = None
+    for k, tap in enumerate(taps):
+        moved = padded if k == half else pltpu.roll(padded, (half - k) % full, 0)
+        term = moved[HALO : HALO + length] * tap
+        total = term if total is None else total + term
+    return total
+
+
+def mixer_kernel(
+    n, x_ref, gain_ref, conv_ref, rec_ref, lat_ref, step_ref, rate_ref, spike_ref,
+    ct_ref, xt_ref, lt_ref, head_gain_ref, exit_c_ref, exit_s_ref, out_ref,
+    w_buf, raw, normed, proj, table_ref, turned_ref, ends_ref,
+    c_all, s_all, y_c, y_s, within, reads, states, got, logs, enter, entered, away, came,
+    own_sems, exit_own, x_own, x_send, x_recv,
+    ring_send, ring_recv, mate_send, mate_recv,
+    exit_send, exit_recv, pass_send, pass_recv,
+    s_out, s_in, l_out, l_in, e_out, e_in, p_out, p_in,
+):
+    chips = n // 2
+    hops = chips - 1
+    me, core, spot, device = ring_spot(n)
+    tp_me = lax.axis_index("tp")
+    mate = me + 1 - 2 * core
+    ways = (device(spot + 1), device(spot - 1))
+    own_rows, width = x_ref.shape
+    length = 2 * own_rows
+    pairs, _, group_cols = w_buf.shape
+    depth = w_buf.shape[1] // n
+    half = depth // 2
+    cw, pw, sw = conv_ref.shape[2] // pairs, 2 * HEAD_DIM, 2 * STATE
+
+    def block_rows(owner):
+        return pl.ds(pl.multiple_of(owner * depth, depth), depth)
+
+    own = []
+    for g in range(pairs):
+        offset = 0
+        for ref, wide in ((conv_ref, cw), (rec_ref, pw), (lat_ref, sw)):
+            for i in range(ref.shape[0]):
+                own.append(
+                    pltpu.make_async_copy(
+                        ref.at[i, :, pl.ds(g * wide, wide)],
+                        w_buf.at[g, block_rows(me), pl.ds(offset, wide)],
+                        own_sems.at[len(own)],
+                    )
+                )
+                offset += wide
+    per_group = len(own) // pairs
+    for copy in own:
+        copy.start()
+
+    up, down = (me + 1) % n, (me + n - 1) % n
+    barrier = pltpu.get_barrier_semaphore()
+    greeted = [{"sp": (me + k) % n} for k in range(1, n)]
+    greeted += [{"sp": other, "tp": 1 - tp_me} for other in (me, up, down)]
+    for other in greeted:
+        pl.semaphore_signal(
+            barrier, inc=1, device_id=other, device_id_type=pl.DeviceIdType.MESH
+        )
+    pl.semaphore_wait(barrier, len(greeted))
+
+    def owner_of(step, way):
+        return device(spot - step if way == 0 else spot + step)
+
+    def part_of(g, owner, way):
+        return w_buf.at[g, pl.ds(pl.multiple_of(owner * depth + way * half, half), half), :]
+
+    def ring_copy(g, step, way, shift=0):
+        part = part_of(g, owner_of(step + shift, way), way)
+        at = (g, step, way)
+        return send_to(part, part, ring_send.at[at], ring_recv.at[at], {"sp": ways[way]})
+
+    def mate_copy(g, step, way, incoming=False):
+        owner = owner_of(step, way)
+        part = part_of(g, owner + 1 - 2 * core if incoming else owner, way)
+        at = (g, step, way)
+        return send_to(part, part, mate_send.at[at], mate_recv.at[at], {"sp": mate})
+
+    def start_group(g):
+        for copy in own[g * per_group : (g + 1) * per_group]:
+            copy.wait()
+        for way in range(2):
+            ring_copy(g, 0, way).start()
+        for way in range(2):
+            mate_copy(g, 0, way).start()
+
+    def advance_group(g, step):
+        for way in range(2):
+            ring_copy(g, step, way, 1).wait_recv()
+            if step < hops - 1:
+                ring_copy(g, step + 1, way).start()
+            mate_copy(g, step + 1, way).start()
+
+    turn = 1 - 2 * core
+    exit_refs, exit_alls = (exit_c_ref, exit_s_ref), (c_all, s_all)
+    exit_wide = exit_c_ref.shape[1]
+
+    def exit_cols(which, owner):
+        return exit_alls[which].at[:, pl.ds(pl.multiple_of(owner * exit_wide, exit_wide), exit_wide)]
+
+    def exit_source(which, step):
+        if step == 0:
+            return exit_refs[which]
+        return exit_cols(which, device(spot - turn * step))
+
+    def exit_copy(which, step, shift=0):
+        there = exit_cols(which, device(spot - turn * (step + shift)))
+        src = there if shift else exit_source(which, step)
+        at = (step, which)
+        return send_to(
+            src, there, exit_send.at[at], exit_recv.at[at], {"sp": device(spot + turn)}
+        )
+
+    def pass_copy(which, step, incoming=False):
+        if incoming:
+            there = exit_cols(which, device(spot + turn * step) + 1 - 2 * core)
+            src = there
+        else:
+            there = exit_cols(which, device(spot - turn * step))
+            src = exit_source(which, step)
+        at = (step, which)
+        return send_to(src, there, pass_send.at[at], pass_recv.at[at], {"sp": mate})
+
+    exit_own_copies = [
+        pltpu.make_async_copy(exit_refs[which], exit_cols(which, me), exit_own.at[which])
+        for which in range(2)
+    ]
+
+    def start_exit():
+        for which in range(2):
+            exit_copy(which, 0).start()
+        for which in range(2):
+            pass_copy(which, 0).start()
+            exit_own_copies[which].start()
+
+    def advance_exit(step):
+        for which in range(2):
+            exit_copy(which, step, 1).wait_recv()
+            if step < hops - 1:
+                exit_copy(which, step + 1).start()
+            pass_copy(which, step + 1).start()
+
+    start_group(0)
+    mine = pl.ds(pl.multiple_of(HALO + own_rows * tp_me, HALO), own_rows)
+    across = send_to(x_ref, raw.at[mine], x_send.at[0], x_recv.at[0], {"tp": 1 - tp_me})
+    across.start()
+    here = pltpu.make_async_copy(x_ref, raw.at[mine], x_own)
+    here.start()
+    before, after = pl.ds(0, HALO), pl.ds(HALO + length, HALO)
+
+    def halo(t, low):
+        if low:
+            return send_to(
+                x_ref.at[pl.ds(own_rows - HALO, HALO)], raw.at[before],
+                x_send.at[1 + t], x_recv.at[1], {"sp": up, "tp": t},
+            )
+        return send_to(
+            x_ref.at[pl.ds(0, HALO)], raw.at[after],
+            x_send.at[1 + t], x_recv.at[2], {"sp": down, "tp": t},
+        )
+
+    sends_up = jnp.logical_and(tp_me == 1, me < n - 1)
+    sends_down = jnp.logical_and(tp_me == 0, me > 0)
+
+    @pl.when(sends_up)
+    def _():
+        for t in range(2):
+            halo(t, True).start()
+
+    @pl.when(sends_down)
+    def _():
+        for t in range(2):
+            halo(t, False).start()
+
+    @pl.when(me == 0)
+    def _():
+        raw[0:HALO, :] = jnp.zeros((HALO, width), BF16)
+
+    @pl.when(me == n - 1)
+    def _():
+        raw[HALO + length :, :] = jnp.zeros((HALO, width), BF16)
+
+    def make_normed():
+        here.wait()
+        across.wait()
+
+        @pl.when(me > 0)
+        def _():
+            halo(0, True).wait_recv()
+
+        @pl.when(me < n - 1)
+        def _():
+            halo(0, False).wait_recv()
+
+        @pl.when(sends_up)
+        def _():
+            for t in range(2):
+                halo(t, True).wait_send()
+
+        @pl.when(sends_down)
+        def _():
+            for t in range(2):
+                halo(t, False).wait_send()
+
+        gain = gain_ref[...].astype(F32)
+        tall = 2 * HALO
+
+        def norm_block(i, _):
+            at = pl.ds(pl.multiple_of(i * tall, tall), tall)
+            x32 = raw[at, :].astype(F32)
+            scale = lax.rsqrt(jnp.mean(x32 * x32, axis=-1, keepdims=True) + epsilon)
+            normed[at, :] = (x32 * scale * gain).astype(BF16)
+            return 0
+
+        lax.fori_loop(0, raw.shape[0] // tall, norm_block, 0)
+
+    def make_tables():
+        heads = spike_ref.shape[0]
+        raw_step = lax.dot_general(
+            normed[HALO : HALO + length, :], step_ref[...],
+            (((1,), (1,)), ((), ())), preferred_element_type=F32,
+        ).astype(BF16)
+        lanes = table_ref.shape[1]
+        row = lax.broadcasted_iota(jnp.int32, (2 * heads, lanes), 0)
+        col = lax.broadcasted_iota(jnp.int32, (2 * heads, lanes), 1)
+        pick = jnp.where((row % heads == col // 4) & (row // heads == col % 2), 1.0, 0.0)
+        head_row = lax.broadcasted_iota(jnp.int32, (heads, lanes), 0)
+        head_col = lax.broadcasted_iota(jnp.int32, (heads, lanes), 1)
+        spread = jnp.where(head_row == head_col // 4, 1.0, 0.0).astype(F32)
+        deltas = softplus(jnp.dot(raw_step, pick.astype(BF16), preferred_element_type=F32))
+        rates = jnp.dot(rate_ref[...], spread, precision=HIGHEST, preferred_element_type=F32)
+        side = lax.broadcasted_iota(jnp.int32, (2, lanes), 0)
+        kind2 = lax.broadcasted_iota(jnp.int32, (2, lanes), 1) % 2
+        rates = jnp.sum(jnp.where(side == kind2, rates, 0.0), axis=0, keepdims=True)
+        spikes = lax.dot_general(
+            spike_ref[...], spread, (((0,), (0,)), ((), ())),
+            precision=HIGHEST, preferred_element_type=F32,
+        )
+        logs = spikes - deltas * rates
+        t_at = lax.broadcasted_iota(jnp.int32, (length, length), 0)
+        s_at = lax.broadcasted_iota(jnp.int32, (length, length), 1)
+        tri = jnp.where(t_at >= s_at, 1.0, 0.0).astype(F32)
+        run_f = jnp.dot(tri, logs, precision=HIGHEST, preferred_element_type=F32)
+        tri = jnp.where(t_at <= s_at, 1.0, 0.0).astype(F32)
+        run_b = jnp.dot(tri, logs, precision=HIGHEST, preferred_element_type=F32)
+        kind = lax.broadcasted_iota(jnp.int32, (length, lanes), 1) % 4
+        table = jnp.where(kind < 2, deltas, jnp.where(kind == 2, run_f, run_b))
+        table_ref[...] = table
+        turned_ref[...] = table.T
+        ends = jnp.where(kind[0:1] == 2, run_f[length - 1 : length], run_b[0:1])
+        ends_ref[...] = jnp.broadcast_to(ends, ends_ref.shape)
+
+    def project_group(g):
+        def arrived(step, _):
+            for way in range(2):
+                mate_copy(g, step, way, True).wait_recv()
+            return 0
+
+        lax.fori_loop(0, chips, arrived, 0)
+        tile = group_cols // 3
+
+        def project_tile(i, _):
+            cols = pl.ds(pl.multiple_of(i * tile, STATE), tile)
+            proj[g, :, cols] = jnp.dot(
+                normed[...], w_buf[g, :, cols], preferred_element_type=F32
+            ).astype(BF16)
+            return 0
+
+        lax.fori_loop(0, 3, project_tile, 0)
+
+    def log_copy(k, incoming=False):
+        there = (me + n - k) % n if incoming else (me + k) % n
+        slot = there if incoming else me
+        return send_to(ends_ref, logs.at[slot], l_out.at[k], l_in.at[k], {"sp": there})
+
+    inner = slice(HALO, HALO + length)
+    at_ig, at_va, at_gate = cw, 2 * cw, 3 * cw
+    at_x = at_gate + pw
+    at_b = at_x + pw
+    at_c = at_b + sw
+
+    def rows_f32(j, wide, base):
+        return proj[j, :, base : base + wide].astype(F32)
+
+    def state_copy(owner):
+        return send_to(
+            states.at[owner], got.at[me], s_out.at[owner], s_in.at[me], {"sp": owner}
+        )
+
+    def mix_pair(j):
+        t_at = lax.broadcasted_iota(jnp.int32, (length, length), 0)
+        s_at = lax.broadcasted_iota(jnp.int32, (length, length), 1)
+        below, above = t_at > s_at, t_at < s_at
+        taps = ct_ref[:, j * cw : (j + 1) * cw].astype(F32)
+        gated = rows_f32(j, cw, at_ig) * rows_f32(j, cw, at_va)
+        conv = tap_sum(
+            gated.astype(BF16).astype(F32), [taps[k : k + 1] for k in range(taps.shape[0])], length
+        )
+        og = proj[j, inner, 0:cw].astype(F32)
+        y_c[:, j * cw : (j + 1) * cw] = (og * conv).astype(BF16)
+        taps = xt_ref[:, j * pw : (j + 1) * pw].astype(F32)
+        xs = silu(
+            tap_sum(
+                rows_f32(j, pw, at_x), [taps[k : k + 1] for k in range(taps.shape[0])], length
+            )
+        ).astype(BF16)
+        taps = [lt_ref[k, :, j * sw : (j + 1) * sw].astype(F32) for k in range(lt_ref.shape[0])]
+        bs = silu(
+            tap_sum(rows_f32(j, sw, at_b), [tap[0:1] for tap in taps], length)
+        ).astype(BF16)
+        cs = silu(
+            tap_sum(rows_f32(j, sw, at_c), [tap[1:2] for tap in taps], length)
+        ).astype(BF16)
+        reads[:, j * sw : (j + 1) * sw] = cs
+        outs = []
+        for h in range(2):
+            c_h = cs[:, h * STATE : (h + 1) * STATE]
+            b_h = bs[:, h * STATE : (h + 1) * STATE]
+            x_h = xs[:, h * HEAD_DIM : (h + 1) * HEAD_DIM]
+            head = 2 * j + h
+            cols = table_ref[:, 4 * head : 4 * head + 4]
+            rows = turned_ref[4 * head : 4 * head + 4, :]
+            scores = lax.dot_general(
+                c_h, b_h, (((1,), (1,)), ((), ())), preferred_element_type=F32
+            )
+            gap = jnp.where(above, cols[:, 3:4] - rows[3:4], cols[:, 2:3] - rows[2:3])
+            d_f, d_b = rows[0:1], rows[1:2]
+            scale = jnp.where(below, d_f, jnp.where(above, d_b, d_f + d_b))
+            w = (scores * jnp.exp(gap) * scale).astype(BF16)
+            outs.append(jnp.dot(w, x_h, preferred_element_type=F32))
+            x32 = x_h.astype(F32)
+            end_f = jnp.exp(rows[2:3, length - 1 : length] - cols[:, 2:3])
+            end_b = jnp.exp(rows[3:4, 0:1] - cols[:, 3:4])
+            both = jnp.concatenate(
+                [x32 * (end_f * cols[:, 0:1]), x32 * (end_b * cols[:, 1:2])], axis=1
+            ).astype(BF16)
+            state = lax.dot_general(
+                both, b_h, (((0,), (0,)), ((), ())), preferred_element_type=F32
+            ).astype(BF16)
+            for d in range(2):
+                states[2 * head + d] = state[d * HEAD_DIM : (d + 1) * HEAD_DIM]
+        within[:, j * pw : (j + 1) * pw] = jnp.concatenate(outs, axis=1)
+
+    def send_states(j):
+        for owner in range(4 * j, 4 * j + 4):
+            @pl.when(me != owner)
+            def _():
+                state_copy(owner).start()
+
+            @pl.when(me == owner)
+            def _():
+                got[owner] = states[owner]
+
+    def send_logs():
+        for k in range(1, n):
+            log_copy(k).start()
+        logs[me] = ends_ref[...]
+
+    def project_then(g):
+        return lambda: project_group(g)
+
+    def mix_then(g):
+        def run():
+            mix_pair(g)
+            send_states(g)
+
+        return run
+
+    units = {LAG + 1: make_normed, LAG + 2: make_tables, LAG + 3: send_logs}
+    for g in range(pairs):
+        units[SKEW * g + hops] = project_then(g)
+        units[SKEW * g + hops + 1] = mix_then(g)
+    exit_slot = SKEW * (pairs - 1) + hops - 1
+    last_mix = SKEW * (pairs - 1) + hops + 1
+
+    def slot(t):
+        for g in range(pairs):
+            if g > 0 and t == SKEW * g - 1:
+                start_group(g)
+            if 0 <= t - SKEW * g < hops:
+                advance_group(g, t - SKEW * g)
+        if t == exit_slot - 1:
+            start_exit()
+        if 0 <= t - exit_slot < hops:
+            advance_exit(t - exit_slot)
+        if t in units:
+            units[t]()
+
+    for t in range(last_mix + 2):
+        slot(t)
+
+    for k in range(1, n):
+        log_copy(k, True).wait_recv()
+    lane = 4 * (me // 2) + 2 + me % 2
+    lane_at = lax.broadcasted_iota(jnp.int32, (1, STATE), 1)
+    for k in range(1, n):
+        other = (me + k) % n
+        send_to(
+            states.at[other], got.at[other], s_out.at[other], s_in.at[other], {"sp": other}
+        ).wait_recv()
+    back = me % 2
+    acc = jnp.zeros(got.shape[1:], F32)
+    for i in range(n):
+        j = back * (n - 1 - i) + (1 - back) * i
+        enter[j] = acc.astype(BF16)
+        log = jnp.sum(
+            jnp.where(lane_at == lane, logs[j][0:1, :], 0.0), axis=1, keepdims=True
+        )
+        acc = acc * jnp.exp(log) + got[j].astype(F32)
+    entered[me] = enter[me]
+
+    def enter_copy(k, incoming=False):
+        there = (me + n - k) % n if incoming else (me + k) % n
+        slot = there if incoming else me
+        return send_to(enter.at[there], entered.at[slot], e_out.at[k], e_in.at[k], {"sp": there})
+
+    for k in range(1, n):
+        enter_copy(k).start()
+    for t in range(last_mix + 2, exit_slot + hops):
+        slot(t)
+    for k in range(1, n):
+        enter_copy(k, True).wait_recv()
+
+    for j in range(pairs):
+        outs = []
+        gate = silu(rows_f32(j, pw, at_gate)[inner])
+        for h in range(2):
+            head = 2 * j + h
+            cols = table_ref[:, 4 * head : 4 * head + 4]
+            wide = jnp.concatenate([entered[2 * head], entered[2 * head + 1]], axis=0)
+            both = lax.dot_general(
+                reads[:, head * STATE : (head + 1) * STATE], wide,
+                (((1,), (1,)), ((), ())), preferred_element_type=F32,
+            )
+            mine = slice(h * HEAD_DIM, (h + 1) * HEAD_DIM)
+            y = within[:, head * HEAD_DIM : (head + 1) * HEAD_DIM]
+            y = y + both[:, :HEAD_DIM] * jnp.exp(cols[:, 2:3])
+            y = y + both[:, HEAD_DIM:] * jnp.exp(cols[:, 3:4])
+            g = y * gate[:, mine]
+            g = g * lax.rsqrt(jnp.mean(g * g, axis=-1, keepdims=True) + epsilon)
+            gain = head_gain_ref[:, head * HEAD_DIM : (head + 1) * HEAD_DIM].astype(F32)
+            outs.append(g * gain)
+        y_s[:, j * pw : (j + 1) * pw] = jnp.concatenate(outs, axis=1).astype(BF16)
+    for which in range(2):
+        exit_own_copies[which].wait()
+        for step in range(chips):
+            pass_copy(which, step, True).wait_recv()
+
+    part = width // BLOCKS
+
+    def partial(owner, block):
+        rows = pl.ds(pl.multiple_of(owner * own_rows, HALO), own_rows)
+        cols = slice(block * part, (block + 1) * part)
+        return jnp.dot(
+            y_c[rows, :], c_all[:, cols], preferred_element_type=F32
+        ) + jnp.dot(y_s[rows, :], s_all[:, cols], preferred_element_type=F32)
+
+    def partial_copy(block):
+        return send_to(
+            away.at[block], came.at[block], p_out.at[block], p_in.at[block], {"tp": 1 - tp_me}
+        )
+
+    for block in range(BLOCKS):
+        away[block] = partial(1 - tp_me, block).astype(BF16)
+        partial_copy(block).start()
+    for block in range(BLOCKS):
+        kept = partial(tp_me, block)
+        partial_copy(block).wait_recv()
+        cols = slice(block * part, (block + 1) * part)
+        out_ref[:, cols] = (kept + came[block].astype(F32)).astype(BF16)
+    for block in range(BLOCKS):
+        partial_copy(block).wait_send()
+    for k in range(1, n):
+        log_copy(k).wait_send()
+        enter_copy(k).wait_send()
+        other = (me + k) % n
+        state_copy(other).wait_send()
+    for step in range(chips):
+        for which in range(2):
+            if step < hops:
+                exit_copy(which, step).wait_send()
+            pass_copy(which, step).wait_send()
+
+    def drain(step, _):
+        for g in range(pairs):
+            for way in range(2):
+                @pl.when(step < hops)
+                def _():
+                    ring_copy(g, step, way).wait_send()
+
+                mate_copy(g, step, way).wait_send()
+        return 0
+
+    lax.fori_loop(0, chips, drain, 0)
+
+
+def mixer(
+    rows, gain, conv_w, rec_w, lat_w, step_w, rate, spike,
+    conv_taps, x_taps, latent_taps, head_gain, exit_c, exit_s,
+):
+    n = lax.axis_size("sp")
+    chips = n // 2
+    hops = chips - 1
+    own_rows, width = rows.shape
+    length = 2 * own_rows
+    full = length + 2 * HALO
+    depth = conv_w.shape[1]
+    blocks = sum(w.shape[0] for w in (conv_w, rec_w, lat_w))
+    cols = sum(w.shape[0] * w.shape[2] for w in (conv_w, rec_w, lat_w))
+    heads = spike.shape[0]
+    pairs = heads // 2
+    conv_width, ssd_width = exit_c.shape[0], exit_s.shape[0]
+    state_width = latent_taps.shape[2]
+    assert 4 * heads <= STATE and 2 * heads == n and conv_width == ssd_width
+    vmem = pl.BlockSpec(memory_space=pltpu.VMEM)
+    hbm = pl.BlockSpec(memory_space=pl.ANY)
+    spans = (n, HEAD_DIM, STATE)
+    parts = (BLOCKS, own_rows, width // BLOCKS)
+    dma = pltpu.SemaphoreType.DMA
+    return pl.pallas_call(
+        functools.partial(mixer_kernel, n),
+        out_shape=jax.ShapeDtypeStruct((own_rows, width), BF16),
+        in_specs=[vmem, vmem, hbm, hbm, hbm] + [vmem] * 9,
+        out_specs=vmem,
+        scratch_shapes=[
+            pltpu.VMEM((pairs, n * depth, cols // pairs), BF16),
+            pltpu.VMEM((full, width), BF16),
+            pltpu.VMEM((full, width), BF16),
+            pltpu.VMEM((pairs, full, cols // pairs), BF16),
+            pltpu.VMEM((length, STATE), F32),
+            pltpu.VMEM((STATE, length), F32),
+            pltpu.VMEM((8, STATE), F32),
+            pltpu.VMEM((conv_width, width), BF16),
+            pltpu.VMEM((ssd_width, width), BF16),
+            pltpu.VMEM((length, conv_width), BF16),
+            pltpu.VMEM((length, ssd_width), BF16),
+            pltpu.VMEM((length, ssd_width), F32),
+            pltpu.VMEM((length, state_width), BF16),
+            pltpu.VMEM(spans, BF16),
+            pltpu.VMEM(spans, BF16),
+            pltpu.VMEM((n, 8, STATE), F32),
+            pltpu.VMEM(spans, BF16),
+            pltpu.VMEM(spans, BF16),
+            pltpu.VMEM(parts, BF16),
+            pltpu.VMEM(parts, BF16),
+            dma((pairs * blocks,)), dma((2,)), dma, dma((3,)), dma((3,)),
+            dma((pairs, hops, 2)), dma((pairs, hops, 2)),
+            dma((pairs, chips, 2)), dma((pairs, chips, 2)),
+            dma((hops, 2)), dma((hops, 2)), dma((chips, 2)), dma((chips, 2)),
+        ]
+        + [dma((n,))] * 6
+        + [dma((BLOCKS,))] * 2,
+        compiler_params=pltpu.CompilerParams(
+            collective_id=2, has_side_effects=True, vmem_limit_bytes=58 * 2**20
+        ),
+        cost_estimate=pl.CostEstimate(
+            flops=2 * full * width * cols, bytes_accessed=2 * width * cols, transcendentals=0
+        ),
+    )(
+        rows, gain.reshape(1, -1), conv_w, rec_w, lat_w, step_w, rate, spike,
+        conv_taps, x_taps, latent_taps, head_gain.reshape(1, -1), exit_c, exit_s,
+    )
+
+
 def project_kernel(r_ref, w_ref, o_ref):
     o_ref[...] = jnp.dot(r_ref[...], w_ref[...], preferred_element_type=F32).astype(BF16)
 
@@ -329,6 +931,17 @@
     pairs = heads // 2
     cw = conv_width // pairs
 
+    share = heads * 2 * HEAD_DIM // n
+    if tp == 2 and 2 * heads == n:
+        return mixer(
+            layer_source_rows, entry_rescale_factor, sliding_mixer_entry_matrix,
+            recurrent_mixer_entry_matrix, latent_write_read_matrix,
+            timestep_matrix.transpose(1, 2, 0).reshape(2 * heads, width),
+            lane_forgetting_rate, spike_forgetting_rate.T, sliding_kernel_coefficients,
+            recurrent_kernel_coefficients, latent_kernel_coefficients, lane_rescale_factor,
+            sliding_mixer_exit_matrix, recurrent_mixer_exit_matrix,
+        )
+
     block = jnp.concatenate(
         [sliding_mixer_entry_matrix[i] for i in range(3)]
         + [recurrent_mixer_entry_matrix[i] for i in range(2)]
@@ -368,8 +981,6 @@
     col_table = table.reshape(length, pairs, 8).transpose(1, 0, 2)
     row_table = table.reshape(length, pairs, 8).transpose(1, 2, 0)
     span_log = jnp.stack([run_f[length - 1], run_b[0]], axis=1)
-    share = heads * 2 * HEAD_DIM // n
-
     exit_c, exit_s, weights = lax.optimization_barrier(
         (sliding_mixer_exit_matrix, recurrent_mixer_exit_matrix, weights)
     )

time: 240 us -> 171 us (0.71); the launches traced: 237 us -> 171 us
  waiting for transfers between devices: 39.3 us -> 0 us
  Pallas kernels: 148 us -> 167 us
  between operations: 13.4 us -> 0.01 us
  matrix products: 11.3 us -> 0 us
  local copies, waits for them, and re-layouts: 12.7 us -> 3.98 us
  starting transfers between devices: 7.44 us -> 0 us
  other arithmetic: 4.66 us -> 0 us
    all_gather x3 -> x0, waiting for transfers between devices: 20.3 us -> none  [the longest x1 20.3 us: local(): exit_s = lax.all_gather(exit_s, 'sp', axis=1, tiled=True)]
    pallas_call x5 -> x1, Pallas kernels: 148 us -> 167 us  [mixer(): pl.pallas_call(functools.partial(mixer_kernel, n), out_shape=jax.ShapeDty...]
    ppermute x3 -> x0, waiting for transfers between devices: 18.2 us -> none  [the longest x1 16.7 us: local(): arrived = lax.ppermute(away, 'tp', [(0, 1), (1, 0)])]
    dot_general x7 -> x0, matrix products: 11.3 us -> none  [the longest x2 5.27 us: partial(): jnp.dot(y_s, exit_s, preferred_element_type=F32)]
    ppermute x3 -> x0, starting transfers between devices: 7.36 us -> none  [the longest x1 3.77 us: local(): after = lax.ppermute(normed[:HALO], 'sp', down)]
    unnamed x37 -> x3, local copies, waits for them, and re-layouts: 7.44 us -> 2.09 us
  transfers between devices with their start and end apart: 6 -> 0, of which waited for: 3 -> 0; matrix products, arithmetic and copies ran while one was open for 5% -> 0% of each run, Pallas kernels for 62% -> 0%
where the time goes in v3:
time: 171 us
  Pallas kernels  167 us (98%)
  local copies, waits for them, and re-layouts  3.98 us (2%)
    pallas_call x1, Pallas kernels, mixer(): pl.pallas_call(functools.partial(mixer_kernel, n), out_shape=jax.ShapeDty...  167 us

profile of v3, /device:TPU:12, one launch (start us, length us, event | category | flops | bytes accessed | tf_op | source)
XLA Modules:
  0.0 170.8 jit_solution(3899050509954029050)
XLA Ops:
  0.0 0.0 copy-start
  0.0 1.3 reshape.11.head_gain_ref
  1.3 0.0 copy-done
  1.3 0.6 reshape.9.gain_ref
  1.9 166.9 %shard_map.136 = bf16[192,2048]{1,0:T(8,128)(2,1)} custom-call(bf16[192,2048]{1,0:T(8,128)(2,1)} %x_ref.1, bf16[1,2048]{1,0:T(2,128)(2,1)} %reshape.9.gain_ref, bf16[3,128,512]{2,1,0:T(8,128)(2,1)} %conv_ref.1, bf16[2,128,512]{2,1,0:T(8,128)(2,1)} %rec_ref.1, bf16[2,128,1024]{2,1,0:T(8,128)(2,1)} %lat_ref.1, bf16[16,2048]{1,0:T(8,128)(2,1)} %bitcast.4, ...), custom_call_target="tpu_custom_call" | custom-call | flops 7851737088 | bytes 18874368 | tf_op jit(solution)/shard_map/pallas_call | solution.py:825
  168.8 2.1 %copy.16 = bf16[192,2048]{1,0:T(8,128)(2,1)} copy(bf16[192,2048]{1,0:T(8,128)(2,1)} %shard_map.136) | data formatting | bytes 1572864
Async XLA Ops:
  0.0 1.3 copy-start

commit v4 on v3

--- a/solution.py
+++ b/solution.py
@@ -12,8 +12,10 @@
 HALO = 16
 CHUNKS = 2
 LAG = 2
-SKEW = 2
-BLOCKS = 4
+SKEW = 1
+EXIT_LAG = 6
+AHEAD = 1
+AWAIT = 2
 epsilon = 1e-05
 F32 = jnp.float32
 BF16 = jnp.bfloat16
@@ -507,7 +509,7 @@
             for t in range(2):
                 halo(t, False).wait_send()
 
-        gain = gain_ref[...].astype(F32)
+        gain = gain_ref[...].astype(F32).reshape(1, -1)
         tall = 2 * HALO
 
         def norm_block(i, _):
@@ -671,63 +673,54 @@
 
         return run
 
-    units = {LAG + 1: make_normed, LAG + 2: make_tables, LAG + 3: send_logs}
-    for g in range(pairs):
-        units[SKEW * g + hops] = project_then(g)
-        units[SKEW * g + hops + 1] = mix_then(g)
-    exit_slot = SKEW * (pairs - 1) + hops - 1
-    last_mix = SKEW * (pairs - 1) + hops + 1
-
-    def slot(t):
-        for g in range(pairs):
-            if g > 0 and t == SKEW * g - 1:
-                start_group(g)
-            if 0 <= t - SKEW * g < hops:
-                advance_group(g, t - SKEW * g)
-        if t == exit_slot - 1:
-            start_exit()
-        if 0 <= t - exit_slot < hops:
-            advance_exit(t - exit_slot)
-        if t in units:
-            units[t]()
-
-    for t in range(last_mix + 2):
-        slot(t)
-
-    for k in range(1, n):
-        log_copy(k, True).wait_recv()
-    lane = 4 * (me // 2) + 2 + me % 2
-    lane_at = lax.broadcasted_iota(jnp.int32, (1, STATE), 1)
-    for k in range(1, n):
-        other = (me + k) % n
-        send_to(
-            states.at[other], got.at[other], s_out.at[other], s_in.at[other], {"sp": other}
-        ).wait_recv()
-    back = me % 2
-    acc = jnp.zeros(got.shape[1:], F32)
-    for i in range(n):
-        j = back * (n - 1 - i) + (1 - back) * i
-        enter[j] = acc.astype(BF16)
-        log = jnp.sum(
-            jnp.where(lane_at == lane, logs[j][0:1, :], 0.0), axis=1, keepdims=True
-        )
-        acc = acc * jnp.exp(log) + got[j].astype(F32)
-    entered[me] = enter[me]
-
-    def enter_copy(k, incoming=False):
-        there = (me + n - k) % n if incoming else (me + k) % n
-        slot = there if incoming else me
-        return send_to(enter.at[there], entered.at[slot], e_out.at[k], e_in.at[k], {"sp": there})
-
-    for k in range(1, n):
-        enter_copy(k).start()
-    for t in range(last_mix + 2, exit_slot + hops):
-        slot(t)
-    for k in range(1, n):
-        enter_copy(k, True).wait_recv()
-
-    for j in range(pairs):
+    late = 4 * (pairs - 1)
+
+    def enter_copy(there, owner):
+        return send_to(
+            enter.at[there], entered.at[owner], e_out.at[there], e_in.at[owner], {"sp": there}
+        )
+
+    def scan_states():
+        for k in range(1, n):
+            log_copy(k, True).wait_recv()
+        for k in range(1, n):
+            other = (me + k) % n
+            send_to(
+                states.at[other], got.at[other], s_out.at[other], s_in.at[other], {"sp": other}
+            ).wait_recv()
+        lane = 4 * (me // 2) + 2 + me % 2
+        lane_at = lax.broadcasted_iota(jnp.int32, (1, STATE), 1)
+        back = me % 2
+
+        def scan_one(i, acc):
+            j = back * (n - 1 - i) + (1 - back) * i
+            enter[j] = acc.astype(BF16)
+            log = jnp.sum(
+                jnp.where(lane_at == lane, logs[j][0:1, :], 0.0), axis=1, keepdims=True
+            )
+            return acc * jnp.exp(log) + got[j].astype(F32)
+
+        acc = jnp.zeros(got.shape[1:], F32)
+        for i in range(n):
+            acc = scan_one(i, acc)
+        entered[me] = enter[me]
+        for k in range(1, n):
+            enter_copy((me + k) % n, me).start()
+
+    def scan_early():
+        pl.when(me < late)(scan_states)
+
+    def scan_late():
+        pl.when(me >= late)(scan_states)
+
+    def finish_pair(j):
+        for owner in range(4 * j, 4 * j + 4):
+            @pl.when(me != owner)
+            def _():
+                enter_copy(me, owner).wait_recv()
+
         outs = []
+        gains = head_gain_ref[...].astype(F32).reshape(1, -1)
         gate = silu(rows_f32(j, pw, at_gate)[inner])
         for h in range(2):
             head = 2 * j + h
@@ -743,42 +736,92 @@
             y = y + both[:, HEAD_DIM:] * jnp.exp(cols[:, 3:4])
             g = y * gate[:, mine]
             g = g * lax.rsqrt(jnp.mean(g * g, axis=-1, keepdims=True) + epsilon)
-            gain = head_gain_ref[:, head * HEAD_DIM : (head + 1) * HEAD_DIM].astype(F32)
+            gain = gains[:, head * HEAD_DIM : (head + 1) * HEAD_DIM]
             outs.append(g * gain)
         y_s[:, j * pw : (j + 1) * pw] = jnp.concatenate(outs, axis=1).astype(BF16)
-    for which in range(2):
-        exit_own_copies[which].wait()
-        for step in range(chips):
-            pass_copy(which, step, True).wait_recv()
-
-    part = width // BLOCKS
-
-    def partial(owner, block):
+    def finish_then(j):
+        return lambda: finish_pair(j)
+
+    units = {LAG + 1: [make_normed], LAG + 2: [make_tables], LAG + 3: [send_logs]}
+    for g in range(pairs):
+        units.setdefault(SKEW * g + hops, []).append(project_then(g))
+        units.setdefault(SKEW * g + hops + 1, []).insert(0, mix_then(g))
+    exit_slot = SKEW * (pairs - 1) + EXIT_LAG
+    last_mix = SKEW * (pairs - 1) + hops + 1
+
+    def slot(t):
+        for g in range(pairs):
+            if g > 0 and t == max(SKEW * g - AHEAD, 0):
+                start_group(g)
+            if 0 <= t - SKEW * g < hops:
+                advance_group(g, t - SKEW * g)
+        if t == exit_slot - 1:
+            start_exit()
+        if 0 <= t - exit_slot < hops:
+            advance_exit(t - exit_slot)
+        for unit in units.get(t, []):
+            unit()
+
+    scan_slot = SKEW * (pairs - 1) + hops
+    units[scan_slot].append(scan_early)
+    for j in range(pairs - 1):
+        units.setdefault(last_mix + 1, []).append(finish_then(j))
+    for t in range(last_mix + 2):
+        slot(t)
+    scan_late()
+    def partial(owner, place):
         rows = pl.ds(pl.multiple_of(owner * own_rows, HALO), own_rows)
-        cols = slice(block * part, (block + 1) * part)
+        cols = pl.ds(pl.multiple_of(place * exit_wide, exit_wide), exit_wide)
         return jnp.dot(
             y_c[rows, :], c_all[:, cols], preferred_element_type=F32
         ) + jnp.dot(y_s[rows, :], s_all[:, cols], preferred_element_type=F32)
 
-    def partial_copy(block):
+    def place_of(step, passed):
+        if passed:
+            return device(spot + turn * step) + 1 - 2 * core
+        return device(spot - turn * step)
+
+    def partial_copy(step, passed):
+        at = 2 * step + passed
         return send_to(
-            away.at[block], came.at[block], p_out.at[block], p_in.at[block], {"tp": 1 - tp_me}
-        )
-
-    for block in range(BLOCKS):
-        away[block] = partial(1 - tp_me, block).astype(BF16)
-        partial_copy(block).start()
-    for block in range(BLOCKS):
-        kept = partial(tp_me, block)
-        partial_copy(block).wait_recv()
-        cols = slice(block * part, (block + 1) * part)
-        out_ref[:, cols] = (kept + came[block].astype(F32)).astype(BF16)
-    for block in range(BLOCKS):
-        partial_copy(block).wait_send()
+            away.at[at], came.at[at], p_out.at[at], p_in.at[at], {"tp": 1 - tp_me}
+        )
+
+    def send_blocks(step):
+        for passed in range(2):
+            for which in range(2):
+                if passed:
+                    pass_copy(which, step, True).wait_recv()
+                elif step == 0:
+                    exit_own_copies[which].wait()
+            away[2 * step + passed] = partial(1 - tp_me, place_of(step, passed)).astype(BF16)
+            partial_copy(step, passed).start()
+
+    rest = list(range(last_mix + 2, exit_slot + hops))
+    for t in rest[:AWAIT]:
+        slot(t)
+    finish_pair(pairs - 1)
+    done = min(hops, max(exit_slot + hops - len(rest[AWAIT:]) - exit_slot, 0))
+    for step in range(done):
+        send_blocks(step)
+    for t in rest[AWAIT:]:
+        slot(t)
+        send_blocks(t - exit_slot)
+    send_blocks(hops)
+    for step in range(chips):
+        for passed in range(2):
+            place = place_of(step, passed)
+            kept = partial(tp_me, place)
+            partial_copy(step, passed).wait_recv()
+            cols = pl.ds(pl.multiple_of(place * exit_wide, exit_wide), exit_wide)
+            out_ref[:, cols] = (kept + came[2 * step + passed].astype(F32)).astype(BF16)
+    for step in range(chips):
+        for passed in range(2):
+            partial_copy(step, passed).wait_send()
     for k in range(1, n):
         log_copy(k).wait_send()
-        enter_copy(k).wait_send()
         other = (me + k) % n
+        enter_copy(other, me).wait_send()
         state_copy(other).wait_send()
     for step in range(chips):
         for which in range(2):
@@ -820,12 +863,12 @@
     vmem = pl.BlockSpec(memory_space=pltpu.VMEM)
     hbm = pl.BlockSpec(memory_space=pl.ANY)
     spans = (n, HEAD_DIM, STATE)
-    parts = (BLOCKS, own_rows, width // BLOCKS)
+    parts = (n, own_rows, width // n)
     dma = pltpu.SemaphoreType.DMA
     return pl.pallas_call(
         functools.partial(mixer_kernel, n),
         out_shape=jax.ShapeDtypeStruct((own_rows, width), BF16),
-        in_specs=[vmem, vmem, hbm, hbm, hbm] + [vmem] * 9,
+        in_specs=[hbm, vmem, hbm, hbm, hbm] + [vmem] * 7 + [hbm] * 2,
         out_specs=vmem,
         scratch_shapes=[
             pltpu.VMEM((pairs, n * depth, cols // pairs), BF16),
@@ -854,7 +897,7 @@
             dma((hops, 2)), dma((hops, 2)), dma((chips, 2)), dma((chips, 2)),
         ]
         + [dma((n,))] * 6
-        + [dma((BLOCKS,))] * 2,
+        + [dma((n,))] * 2,
         compiler_params=pltpu.CompilerParams(
             collective_id=2, has_side_effects=True, vmem_limit_bytes=58 * 2**20
         ),
@@ -862,8 +905,8 @@
             flops=2 * full * width * cols, bytes_accessed=2 * width * cols, transcendentals=0
         ),
     )(
-        rows, gain.reshape(1, -1), conv_w, rec_w, lat_w, step_w, rate, spike,
-        conv_taps, x_taps, latent_taps, head_gain.reshape(1, -1), exit_c, exit_s,
+        rows, gain, conv_w, rec_w, lat_w, step_w, rate, spike,
+        conv_taps, x_taps, latent_taps, head_gain, exit_c, exit_s,
     )
 
 

time: 171 us -> 164 us (0.959)
  Pallas kernels: 167 us -> 160 us
  local copies, waits for them, and re-layouts: 3.98 us -> 2.09 us
    pallas_call x1, Pallas kernels: 167 us -> 160 us  [mixer(): pl.pallas_call(functools.partial(mixer_kernel, n), out_shape=jax.ShapeDty...]
    reshape x2 -> x0, local copies, waits for them, and re-layouts: 1.89 us -> none  [the longest x1 1.28 us: mixer(): head_gain.reshape(1, -1)]
where the time goes in v4:
time: 164 us; the launch traced here: 162 us
  Pallas kernels  160 us (98%)
  local copies, waits for them, and re-layouts  2.09 us (1%)
    pallas_call x1, Pallas kernels, mixer(): pl.pallas_call(functools.partial(mixer_kernel, n), out_shape=jax.ShapeDty...  160 us

profile of v4, /device:TPU:12, one launch (start us, length us, event | category | flops | bytes accessed | tf_op | source)
XLA Modules:
  0.0 162.3 jit_solution(10877546211546947486)
XLA Ops:
  0.0 160.2 %shard_map.136 = bf16[192,2048]{1,0:T(8,128)(2,1)} custom-call(bf16[192,2048]{1,0:T(8,128)(2,1)} %x_ref.1, bf16[2048]{0:T(1024)(128)(2,1)} %gain_ref.1, bf16[3,128,512]{2,1,0:T(8,128)(2,1)} %conv_ref.1, bf16[2,128,512]{2,1,0:T(8,128)(2,1)} %rec_ref.1, bf16[2,128,1024]{2,1,0:T(8,128)(2,1)} %lat_ref.1, bf16[16,2048]{1,0:T(8,128)(2,1)} %bitcast.4, ...), custom_call_target="tpu_custom_call" | custom-call | flops 7851737088 | bytes 18874368 | tf_op jit(solution)/shard_map/pallas_call | solution.py:868
  160.3 2.1 %copy.16 = bf16[192,2048]{1,0:T(8,128)(2,1)} copy(bf16[192,2048]{1,0:T(8,128)(2,1)} %shard_map.136) | data formatting | bytes 1572864

commit v5 on v4

--- a/solution.py
+++ b/solution.py
@@ -13,7 +13,7 @@
 CHUNKS = 2
 LAG = 2
 SKEW = 1
-EXIT_LAG = 6
+EXIT_LAG = 7
 AHEAD = 1
 AWAIT = 2
 epsilon = 1e-05
@@ -235,7 +235,7 @@
     for i in range(n):
         j = back * (n - 1 - i) + (1 - back) * i
         enter[j] = acc.astype(BF16)
-        acc = acc * jnp.exp(logs[j][0:1, :]) + got[j].astype(F32)
+        acc = acc * jnp.exp(logs[j, 0:1]) + got[j].astype(F32)
     out_ref[me] = enter[me]
     for k in range(1, n):
         copy(enter, out_ref, e_out, e_in, k, (me + k) % n, me).start()
@@ -578,7 +578,9 @@
     def log_copy(k, incoming=False):
         there = (me + n - k) % n if incoming else (me + k) % n
         slot = there if incoming else me
-        return send_to(ends_ref, logs.at[slot], l_out.at[k], l_in.at[k], {"sp": there})
+        return send_to(
+            ends_ref.at[pl.ds(0, 1)], logs.at[slot, pl.ds(0, 1)], l_out.at[k], l_in.at[k], {"sp": there}
+        )
 
     inner = slice(HALO, HALO + length)
     at_ig, at_va, at_gate = cw, 2 * cw, 3 * cw
@@ -661,7 +663,7 @@
     def send_logs():
         for k in range(1, n):
             log_copy(k).start()
-        logs[me] = ends_ref[...]
+        logs[me, 0:1] = ends_ref[0:1, :]
 
     def project_then(g):
         return lambda: project_group(g)
@@ -696,7 +698,7 @@
             j = back * (n - 1 - i) + (1 - back) * i
             enter[j] = acc.astype(BF16)
             log = jnp.sum(
-                jnp.where(lane_at == lane, logs[j][0:1, :], 0.0), axis=1, keepdims=True
+                jnp.where(lane_at == lane, logs[j, 0:1], 0.0), axis=1, keepdims=True
             )
             return acc * jnp.exp(log) + got[j].astype(F32)
 

time: 164 us -> 162 us (0.988)
  no operation moved by 1% of the time
where the time goes in v5:
time: 162 us; the launch traced here: 161 us
  Pallas kernels  159 us (98%)
  local copies, waits for them, and re-layouts  2.09 us (1%)
    pallas_call x1, Pallas kernels, mixer(): pl.pallas_call(functools.partial(mixer_kernel, n), out_shape=jax.ShapeDty...  159 us

profile of v5, /device:TPU:12, one launch (start us, length us, event | category | flops | bytes accessed | tf_op | source)
XLA Modules:
  0.0 160.9 jit_solution(4632094497393616756)
XLA Ops:
  0.0 158.8 %shard_map.136 = bf16[192,2048]{1,0:T(8,128)(2,1)} custom-call(bf16[192,2048]{1,0:T(8,128)(2,1)} %x_ref.1, bf16[2048]{0:T(1024)(128)(2,1)} %gain_ref.1, bf16[3,128,512]{2,1,0:T(8,128)(2,1)} %conv_ref.1, bf16[2,128,512]{2,1,0:T(8,128)(2,1)} %rec_ref.1, bf16[2,128,1024]{2,1,0:T(8,128)(2,1)} %lat_ref.1, bf16[16,2048]{1,0:T(8,128)(2,1)} %bitcast.4, ...), custom_call_target="tpu_custom_call" | custom-call | flops 7851737088 | bytes 18874368 | tf_op jit(solution)/shard_map/pallas_call | solution.py:870
  158.8 2.1 %copy.16 = bf16[192,2048]{1,0:T(8,128)(2,1)} copy(bf16[192,2048]{1,0:T(8,128)(2,1)} %shard_map.136) | data formatting | bytes 1572864
